TPU v7x, 128 devices: a whole 4x4x4 slice. The times are simulated.
128 devices in a mesh: sp: 16 (over z, y), dp: 8 (over x, core).
Axes of the slice: x: 4, y: 4, z: 4, core: 2. Of those that a mesh axis runs over, the one named last changes fastest.
Arguments:
- query_weight: bfloat16 [8, 6144, 1024], P('dp', 'sp'), may hold values from -6 to 6
- forget_preactivation: bfloat16 [8, 6144, 1024], P('dp', 'sp'), may hold values from -7 to 7
- written_input: bfloat16 [8, 6144, 1024], P('dp', 'sp'), may hold values from -6 to 6
- output_gate_logit: bfloat16 [8, 6144, 1024], P('dp', 'sp'), may hold values from -6 to 6
- forget_floor: float32 [1024], replicated, may hold values from 0.9 to 1
- extra_log_decay: float32 [8, 6144, 16], P('dp'), may hold values from -0.7 to 0
- residual: bfloat16 [8, 6144, 2048], P('dp', 'sp'), may hold values from -6 to 6
- output_weight: bfloat16 [1024, 2048], P('dp'), may hold values from -0.1875 to 0.1875
- norm_scale_vector: float32 [2048], replicated, may hold values from 0.1 to 1.9
- expert_gate_weight: bfloat16 [16, 2048, 1024], P('sp'), may hold values from -0.125 to 0.125
- expert_up_weight: bfloat16 [16, 2048, 1024], P('sp'), may hold values from -0.125 to 0.125
- expert_down_weight: bfloat16 [16, 1024, 2048], P('sp'), may hold values from -0.1875 to 0.1875
- routes: int32 [8, 6144, 2], P('dp', 'sp'), may hold values from 0 to 15, as said below
- routing_weight: float32 [8, 6144, 2], P('dp', 'sp'), may hold values from 0.2 to 1
Outputs:
- layer_out: bfloat16 [8, 6144, 2048], P('dp', 'sp')
Inputs may be any that keep to these rules, and one draw needn't show every extreme that they name: `routes`: the two experts of a position differ and lie in one group of four, 4 g to 4 g + 3. In the positions of one device no expert is named more than 96 times. In every draw one expert is named exactly 96 times by the positions of every device, and on some devices each of the four experts of one group is named exactly 96 times.
All inputs are finite; a program needn't handle non-finite values.
Results may differ from a plain program's by a relative error of at most 0.0059.
Values may be sent and summed in bfloat16 or wider, within the bound.
No kernel may reach another device: no remote copies, remote signals or barrier semaphores. Data moves between devices by JAX's collectives and lax.ppermute only.
A program may use at most 128 MiB of HBM per device.

v0:
```python
import functools

import jax
import jax.numpy as jnp
from jax import lax
from jax.experimental import pallas as pl
from jax.experimental.pallas import tpu as pltpu
from jax.sharding import Mesh
from jax.sharding import PartitionSpec as P

CH = 64
BLK = 64
GL = 256
SP = ("sp_0", "sp_1")
DP = ("x", "c")
PACK = 80
F32 = jnp.float32
BF = jnp.bfloat16


def dot(a, b, dims=((1,), (0,))):
    return lax.dot_general(a, b, (dims, ((), ())), preferred_element_type=F32)


def split3(v):
    hi = v.astype(BF)
    rest = v - hi.astype(F32)
    mid = rest.astype(BF)
    low = (rest - mid.astype(F32)).astype(BF)
    return hi, mid, low


def split2(v):
    hi = v.astype(BF)
    return hi, (v - hi.astype(F32)).astype(BF)


def tri(n):
    return (
        lax.broadcasted_iota(jnp.int32, (n, n), 0) >= lax.broadcasted_iota(jnp.int32, (n, n), 1)
    )


def same_head(rows, lanes):
    return (
        lax.broadcasted_iota(jnp.int32, (rows, lanes), 0) // CH
        == lax.broadcasted_iota(jnp.int32, (rows, lanes), 1) // CH
    )


def silu(v):
    return v / (1.0 + jnp.exp(-v))


def keys_and_logs(f_ref, floor_ref, spike_ref, group):
    f = f_ref[...].astype(F32)
    keys = (1.0 - floor_ref[...]) / (1.0 + jnp.exp(f))
    poly = jnp.full_like(keys, 1.0 / 10.0)
    for n in range(9, 0, -1):
        poly = poly * keys + 1.0 / n
    heads = spike_ref.shape[1]
    spread = (
        lax.broadcasted_iota(jnp.int32, (heads, GL), 0)
        == group * (GL // CH) + lax.broadcasted_iota(jnp.int32, (heads, GL), 1) // CH
    ).astype(BF)
    hi, mid, low = split3(spike_ref[...])
    burst = dot(hi, spread) + dot(mid, spread) + dot(low, spread)
    return keys, burst - keys * poly


def running_sum(logs, length):
    lower = tri(length).astype(BF)
    out = []
    for b in range(logs.shape[0] // length):
        hi, mid, low = split3(logs[b * length : (b + 1) * length])
        out.append(dot(lower, hi) + dot(lower, mid) + dot(lower, low))
    return out


def states_kernel(f_ref, v_ref, floor_ref, spike_ref, pack_ref):
    group = pl.program_id(0)
    keys, logs = keys_and_logs(f_ref, floor_ref, spike_ref, group)
    parts = running_sum(logs, 128)
    after = jnp.zeros((1, GL), F32)
    acc = jnp.zeros((GL, GL), F32)
    for b in reversed(range(len(parts))):
        close = parts[b][127:128]
        kc = (keys[b * 128 : (b + 1) * 128] * jnp.exp(after + close - parts[b])).astype(BF)
        acc = acc + dot(v_ref[b * 128 : (b + 1) * 128, :], kc, ((0,), (0,)))
        after = after + close
    acc = jnp.where(same_head(GL, GL), acc, 0.0)
    compact = acc[0:64] + acc[64:128] + acc[128:192] + acc[192:256]
    pack_ref[0:64, :] = compact.astype(BF)
    hi, mid, low = split3(after)
    row = lax.broadcasted_iota(jnp.int32, (16, GL), 0)
    tail = jnp.where(row == 0, hi.astype(F32), 0.0)
    tail = jnp.where(row == 1, mid.astype(F32), tail)
    tail = jnp.where(row == 2, low.astype(F32), tail)
    pack_ref[64:80, :] = tail.astype(BF)


def inside_kernel(q_ref, f_ref, v_ref, floor_ref, spike_ref, out_ref, qrun_ref):
    group = pl.program_id(0)
    keys, logs = keys_and_logs(f_ref, floor_ref, spike_ref, group)
    parts = running_sum(logs, BLK)
    q = silu(q_ref[...].astype(F32))
    head_mask = same_head(GL, GL)
    lane = lax.broadcasted_iota(jnp.int32, (BLK, GL), 1)
    causal = (lane % CH) <= lax.broadcasted_iota(jnp.int32, (BLK, GL), 0)
    before = jnp.zeros((1, GL), F32)
    state = jnp.zeros((GL, GL), F32)
    zero = jnp.zeros((GL, GL), BF)
    for b in range(len(parts)):
        rows = slice(b * BLK, (b + 1) * BLK)
        cum = parts[b]
        close = cum[BLK - 1 : BLK]
        k = keys[rows]
        grow = jnp.exp(-cum)
        qd = q[rows] * jnp.exp(cum)
        qrun_ref[rows, :] = (qd * jnp.exp(before)).astype(BF)
        qd = qd.astype(BF)
        kg = (k * grow).astype(BF)
        v = v_ref[rows, :]
        k4 = jnp.where(head_mask, jnp.concatenate([kg] * 4, axis=0), zero)
        v4 = jnp.where(head_mask, jnp.concatenate([v] * 4, axis=0), zero)
        scores = dot(qd, k4, ((1,), (1,)))
        scores = jnp.where(causal, scores, 0.0).astype(BF)
        out = dot(scores, v4)
        if b > 0:
            out = out + dot(qd, state.astype(BF), ((1,), (1,)))
        out_ref[rows, :] = out
        if b + 1 < len(parts):
            kc = (k * jnp.exp(close - cum)).astype(BF)
            add = jnp.where(head_mask, dot(v, kc, ((0,), (0,))), 0.0)
            state = jnp.exp(close) * state + add
        before = before + close


def total_of(pack_ref):
    return (
        pack_ref[64:65, :].astype(F32)
        + pack_ref[65:66, :].astype(F32)
        + pack_ref[66:67, :].astype(F32)
    )


def row_kernel(pos_ref, own_ref, one_ref, two_ref, three_ref, row_ref, before_ref, btot_ref):
    here = pos_ref[0]
    width = own_ref.shape[1]
    state = jnp.zeros((CH, width), F32)
    total = jnp.zeros((1, width), F32)
    pieces = ((3, three_ref), (2, two_ref), (1, one_ref))
    for n, ref in pieces:
        use = n <= here
        t = jnp.where(use, total_of(ref), 0.0)
        state = jnp.exp(t) * state + jnp.where(use, ref[0:64, :].astype(F32), 0.0)
        total = total + t
    before_ref[...] = state
    btot_ref[...] = jnp.broadcast_to(total, (8, width))
    t = total_of(own_ref)
    state = jnp.exp(t) * state + own_ref[0:64, :].astype(F32)
    total = total + t
    for n, ref in pieces:
        use = n > here
        t = jnp.where(use, total_of(ref), 0.0)
        state = jnp.exp(t) * state + jnp.where(use, ref[0:64, :].astype(F32), 0.0)
        total = total + t
    row_ref[0:64, :] = state.astype(BF)
    hi, mid, low = split3(total)
    row = lax.broadcasted_iota(jnp.int32, (16, width), 0)
    tail = jnp.where(row == 0, hi.astype(F32), 0.0)
    tail = jnp.where(row == 1, mid.astype(F32), tail)
    tail = jnp.where(row == 2, low.astype(F32), tail)
    row_ref[64:80, :] = tail.astype(BF)


def mix_kernel(
    tok_steps,
    half,
    pos_ref,
    out_ref,
    qrun_ref,
    gate_ref,
    res_ref,
    before_ref,
    btot_ref,
    one_ref,
    two_ref,
    three_ref,
    wmine_ref,
    wother_ref,
    scale_ref,
    routes_ref,
    upd_ref,
    send_a_ref,
    send_b_ref,
    w_s,
    state_s,
    norm_s,
    pos_s,
    mem_s,
):
    step = pl.program_id(0)
    width = gate_ref.shape[1]
    groups = width // GL
    tok_rows = routes_ref.shape[1]
    rows = gate_ref.shape[0]

    @pl.when(step == 0)
    def _():
        here = pos_ref[0]
        state = jnp.zeros((CH, width), F32)
        for n, ref in ((3, three_ref), (2, two_ref), (1, one_ref)):
            use = n <= here
            t = jnp.where(use, total_of(ref), 0.0)
            state = jnp.exp(t) * state + jnp.where(use, ref[0:64, :].astype(F32), 0.0)
        state = (jnp.exp(btot_ref[0:1, :]) * state + before_ref[...]).astype(BF)
        mask = same_head(GL, GL)
        for g in range(groups):
            one = state[:, g * GL : (g + 1) * GL]
            state_s[g] = jnp.where(mask, jnp.concatenate([one] * 4, axis=0), jnp.zeros((GL, GL), BF))
        x_here = pos_ref[1]
        core = pos_ref[2]
        piece = wmine_ref.shape[1]
        for n in range(4):
            src = (x_here + 4 - n) % 4
            w_s[pl.ds((2 * src + core) * piece, piece), :] = wmine_ref[n]
            w_s[pl.ds((2 * src + 1 - core) * piece, piece), :] = wother_ref[n]
        experts = mem_s.shape[0]
        e = lax.broadcasted_iota(jnp.int32, (experts, tok_rows), 0)
        member = (e == routes_ref[0:1, :]) | (e == routes_ref[1:2, :])
        mem = jnp.where(member, 1.0, 0.0)
        strict = (
            lax.broadcasted_iota(jnp.int32, (tok_rows, tok_rows), 0)
            < lax.broadcasted_iota(jnp.int32, (tok_rows, tok_rows), 1)
        ).astype(BF)
        place = dot(mem.astype(BF), strict)
        pos_s[...] = jnp.where(member, place.astype(jnp.int32), -1)

    @pl.when(step < tok_steps)
    def _():
        ones = jnp.where(same_head(GL, GL), 1.0, 0.0).astype(BF)
        mixed = []
        for g in range(groups):
            lanes = slice(g * GL, (g + 1) * GL)
            o = out_ref[:, lanes] + dot(qrun_ref[:, lanes], state_s[g], ((1,), (1,)))
            hi, low = split2(o * o)
            mean = (dot(hi, ones) + dot(low, ones)) * (1.0 / CH)
            gate = silu(gate_ref[:, lanes].astype(F32))
            mixed.append((o * lax.rsqrt(mean + 1e-06) * gate).astype(BF))
        mixed = jnp.concatenate(mixed, axis=1)
        upd = (res_ref[...].astype(F32) + dot(mixed, w_s[...])).astype(BF)
        upd_ref[...] = upd
        wide = upd.astype(F32)
        mean = jnp.mean(wide * wide, axis=-1, keepdims=True)
        norm = (wide * lax.rsqrt(mean + 1e-06) * scale_ref[...]).astype(BF)
        norm_s[pl.ds(step * rows, rows), :] = norm

    def send(ref, first, base):
        picks = []
        for i in range(ref.shape[0] // half):
            place = pos_s[pl.ds(first + i, 1), :]
            c = lax.broadcasted_iota(jnp.int32, (half, tok_rows), 0) + base
            picks.append(jnp.where(c == place, 1.0, 0.0).astype(BF))
        ref[...] = dot(jnp.concatenate(picks, axis=0), norm_s[...]).astype(BF)

    per = send_a_ref.shape[0] // half
    blocks = mem_s.shape[0] // per

    @pl.when((step >= tok_steps) & (step < tok_steps + blocks))
    def _():
        send(send_a_ref, (step - tok_steps) * per, 0)

    @pl.when(step >= tok_steps + blocks)
    def _():
        send(send_b_ref, (step - tok_steps - blocks) * per, half)


def combine_kernel(cap, half, base, last, routes_ref, wt_ref, got_ref, acc_ref, out_ref, hi_s, low_s):
    experts = got_ref.shape[0] // half
    tok_rows = routes_ref.shape[0]

    @pl.when(pl.program_id(0) == 0)
    def _():
        lane = lax.broadcasted_iota(jnp.int32, (tok_rows, 128), 1)
        r0 = routes_ref[:, 0:1]
        r1 = routes_ref[:, 1:2]
        oh0 = lane == r0
        oh1 = lane == r1
        mem = jnp.where(oh0 | oh1, 1.0, 0.0).astype(BF)
        strict = (
            lax.broadcasted_iota(jnp.int32, (tok_rows, tok_rows), 0)
            > lax.broadcasted_iota(jnp.int32, (tok_rows, tok_rows), 1)
        ).astype(BF)
        place = dot(strict, mem)
        j = lax.broadcasted_iota(jnp.int32, (tok_rows, experts * half), 1)
        weight = jnp.zeros((tok_rows, experts * half), F32)
        for k, (oh, r) in enumerate(((oh0, r0), (oh1, r1))):
            p = jnp.sum(jnp.where(oh, place, 0.0), axis=1, keepdims=True).astype(jnp.int32) - base
            slot = jnp.where((p >= 0) & (p < half), r * half + p, -1)
            weight = weight + jnp.where(j == slot, wt_ref[:, k : k + 1], 0.0)
        hi, low = split2(weight)
        hi_s[...] = hi
        low_s[...] = low

    got = got_ref[...]
    total = acc_ref[...].astype(F32) + (dot(hi_s[...], got) + dot(low_s[...], got))
    out_ref[...] = total.astype(out_ref.dtype)


def ring(n, size=4):
    return [(i, (i + n) % size) for i in range(size)]


def per_device(
    query_weight,
    forget_preactivation,
    written_input,
    output_gate_logit,
    forget_floor,
    extra_log_decay,
    residual,
    output_weight,
    norm_scale_vector,
    expert_gate_weight,
    expert_up_weight,
    expert_down_weight,
    routes,
    routing_weight,
):
    _, tok, width = query_weight.shape
    model = output_weight.shape[1]
    piece = output_weight.shape[0]
    heads = width // CH
    groups = width // GL
    experts = lax.axis_size(SP)
    cap = 4 * tok // experts
    half = cap // 2
    z = lax.axis_index("sp_0")
    y = lax.axis_index("sp_1")
    x = lax.axis_index("x")
    core = lax.axis_index("c")

    spikes = lax.dynamic_slice_in_dim(extra_log_decay[0], lax.axis_index(SP) * tok, tok, 0)
    q, f, v, gate = (
        a.reshape(tok, width)
        for a in (query_weight, forget_preactivation, written_input, output_gate_logit)
    )
    floor = forget_floor.reshape(1, width)
    scale = norm_scale_vector.reshape(1, model)
    res = residual.reshape(tok, model)

    wpieces = [output_weight] + [lax.ppermute(output_weight, "x", ring(n)) for n in (1, 2, 3)]

    tall = pl.BlockSpec((tok, GL), lambda g: (0, g))
    flat = pl.BlockSpec((1, GL), lambda g: (0, g))
    whole = pl.BlockSpec((tok, heads), lambda g: (0, 0))
    pack = pl.pallas_call(
        states_kernel,
        grid=(groups,),
        in_specs=[tall, tall, flat, whole],
        out_specs=pl.BlockSpec((PACK, GL), lambda g: (0, g)),
        out_shape=jax.ShapeDtypeStruct((PACK, width), BF),
        name="states",
    )(f, v, floor, spikes)

    along_y = [lax.ppermute(pack, "sp_1", ring(n)) for n in (1, 2, 3)]

    inside, qrun = pl.pallas_call(
        inside_kernel,
        grid=(groups,),
        in_specs=[tall, tall, tall, flat, whole],
        out_specs=[tall, tall],
        out_shape=[
            jax.ShapeDtypeStruct((tok, width), F32),
            jax.ShapeDtypeStruct((tok, width), BF),
        ],
        name="inside",
    )(q, f, v, floor, spikes)

    vm = pl.BlockSpec(memory_space=pltpu.VMEM)
    sm = pl.BlockSpec(memory_space=pltpu.SMEM)
    row, before, btot = pl.pallas_call(
        row_kernel,
        in_specs=[sm, vm, vm, vm, vm],
        out_specs=[vm, vm, vm],
        out_shape=[
            jax.ShapeDtypeStruct((PACK, width), BF),
            jax.ShapeDtypeStruct((CH, width), F32),
            jax.ShapeDtypeStruct((8, width), F32),
        ],
        name="row",
    )(y.astype(jnp.int32).reshape(1), pack, *along_y)

    along_z = [lax.ppermute(row, "sp_0", ring(n)) for n in (1, 2, 3)]

    wmine = jnp.stack(wpieces)
    wother = lax.ppermute(wmine, "c", [(0, 1), (1, 0)])

    route_rows = jnp.pad(routes[0].T, ((0, 6), (0, 0)), constant_values=-1)
    place = jnp.stack([z, x, core]).astype(jnp.int32)
    tok_steps = 3
    rows = tok // tok_steps
    send_steps = 4
    send_rows = 2 * experts * half // send_steps
    clip = lambda i: jnp.minimum(i, tok_steps - 1)
    tok_w = pl.BlockSpec((rows, width), lambda i: (clip(i), 0))
    tok_m = pl.BlockSpec((rows, model), lambda i: (clip(i), 0))
    full = lambda a: pl.BlockSpec(a.shape, lambda i: (0,) * a.ndim)


    updated, send_a, send_b = pl.pallas_call(
        functools.partial(mix_kernel, tok_steps, half),
        grid=(tok_steps + send_steps,),
        in_specs=[
            sm,
            tok_w,
            tok_w,
            tok_w,
            tok_m,
            full(before),
            full(btot),
            full(row),
            full(row),
            full(row),
            full(wmine),
            full(wmine),
            full(scale),
            full(route_rows),
        ],
        out_specs=[
            tok_m,
            pl.BlockSpec((send_rows, model), lambda i: (jnp.clip(i - tok_steps, 0, 1), 0)),
            pl.BlockSpec((send_rows, model), lambda i: (jnp.clip(i - tok_steps - 2, 0, 1), 0)),
        ],
        out_shape=[
            jax.ShapeDtypeStruct((tok, model), BF),
            jax.ShapeDtypeStruct((experts * half, model), BF),
            jax.ShapeDtypeStruct((experts * half, model), BF),
        ],
        scratch_shapes=[
            pltpu.VMEM((width, model), BF),
            pltpu.VMEM((groups, GL, GL), BF),
            pltpu.VMEM((tok, model), BF),
            pltpu.VMEM((experts, tok), jnp.int32),
            pltpu.VMEM((experts, tok), jnp.int32),
        ],
        compiler_params=pltpu.CompilerParams(vmem_limit_bytes=50 * 1024 * 1024),
        name="mix",
    )(place, inside, qrun, gate, res, before, btot, *along_z, wmine, wother, scale, route_rows)

    def exchange(a):
        return lax.all_to_all(
            a.reshape(experts, half, model), SP, split_axis=0, concat_axis=0, tiled=True
        ).reshape(experts * half, model)

    def serve(a):
        gated = jnp.dot(a, expert_gate_weight[0], preferred_element_type=F32)
        upward = jnp.dot(a, expert_up_weight[0], preferred_element_type=F32)
        hidden = (jax.nn.silu(gated) * upward).astype(BF)
        return jnp.dot(hidden, expert_down_weight[0], preferred_element_type=F32).astype(BF)

    def combine(got, acc, base, last):
        blk = 512
        return pl.pallas_call(
            functools.partial(combine_kernel, cap, half, base, last),
            grid=(model // blk,),
            in_specs=[
                pl.BlockSpec((tok, 2), lambda i: (0, 0)),
                pl.BlockSpec((tok, 2), lambda i: (0, 0)),
                pl.BlockSpec((experts * half, blk), lambda i: (0, i)),
                pl.BlockSpec((tok, blk), lambda i: (0, i)),
            ],
            out_specs=pl.BlockSpec((tok, blk), lambda i: (0, i)),
            out_shape=jax.ShapeDtypeStruct((tok, model), BF if last else F32),
            scratch_shapes=[pltpu.VMEM((tok, experts * half), BF)] * 2,
            name="combine",
        )(routes[0], routing_weight[0], got, acc)

    in_a = exchange(send_a)
    in_b = exchange(send_b)
    got_a = exchange(serve(in_a))
    got_b = exchange(serve(in_b))
    acc = combine(got_a, updated, 0, False)
    layer_out = combine(got_b, acc, half, True)
    return layer_out.reshape(1, tok, model)


def solution(mesh):
    torus = Mesh(
        mesh.devices.reshape(4, 4, 4, mesh.shape["dp"] // 4), ("sp_0", "sp_1", "x", "c")
    )
    return jax.shard_map(
        per_device,
        mesh=torus,
        in_specs=(
            P(DP, SP, None),
            P(DP, SP, None),
            P(DP, SP, None),
            P(DP, SP, None),
            P(),
            P(DP, None, None),
            P(DP, SP, None),
            P(DP, None),
            P(),
            P(SP, None, None),
            P(SP, None, None),
            P(SP, None, None),
            P(DP, SP, None),
            P(DP, SP, None),
        ),
        out_specs=P(DP, SP, None),
        check_vma=False,
    )
```

profile of v0, /device:TPU:0, one launch (start us, length us, event | category | flops | bytes accessed | tf_op | source)
XLA Modules:
  0.0 279.6 jit_solution(5366310944899157112)
XLA Ops:
  1.6 2.7 collective-permute-start.7
  5.8 9.2 %collective-permute-done.6 = bf16[128,2048]{1,0:T(8,128)(2,1)S(1)} collective-permute-done((bf16[128,2048]{1,0:T(8,128)(2,1)}, bf16[128,2048]{1,0:T(8,128)(2,1)S(1)}, u32[]{:S(2)}, u32[]{:S(2)}) %collective-permute-start.6) | collective-permute-done | bytes 524320 | tf_op jit(solution)/shard_map/ppermute | solution.py:353
  15.0 12.4 %collective-permute-done.7 = bf16[128,2048]{1,0:T(8,128)(2,1)S(1)} collective-permute-done((bf16[128,2048]{1,0:T(8,128)(2,1)}, bf16[128,2048]{1,0:T(8,128)(2,1)S(1)}, u32[]{:S(2)}, u32[]{:S(2)}) %collective-permute-start.7) | collective-permute-done | bytes 524320 | tf_op jit(solution)/shard_map/ppermute | solution.py:353
  31.0 6.9 %states.1.own_ref = bf16[80,1024]{1,0:T(8,128)(2,1)} custom-call(bf16[384,1024]{1,0:T(8,128)(2,1)} %bitcast.68, bf16[384,1024]{1,0:T(8,128)(2,1)} %bitcast.70, f32[1,1024]{1,0:T(1,128)} %bitcast.85, f32[384,16]{1,0:T(8,128)} %bitcast.75), custom_call_target="tpu_custom_call" | custom-call | tf_op jit(solution)/shard_map/states/pallas_call | solution.py:358
  39.5 2.9 %collective-permute-start.1 = (bf16[80,1024]{1,0:T(8,128)(2,1)}, bf16[80,1024]{1,0:T(8,128)(2,1)S(1)}, u32[]{:S(2)}, u32[]{:S(2)}) collective-permute-start(bf16[80,1024]{1,0:T(8,128)(2,1)} %states.1.own_ref), channel_id=1, source_target_pairs={{0,16},{8,24},{16,0},{24,8},{1,17},{9,25},{17,1},{25,9},{2,18},{10... | collective-permute-start | bytes 491528 | tf_op jit(solution)/shard_map/ppermute | solution.py:367
  45.9 4.7 %collective-permute-done.1.two_ref = bf16[80,1024]{1,0:T(8,128)(2,1)S(1)} collective-permute-done((bf16[80,1024]{1,0:T(8,128)(2,1)}, bf16[80,1024]{1,0:T(8,128)(2,1)S(1)}, u32[]{:S(2)}, u32[]{:S(2)}) %collective-permute-start.1) | collective-permute-done | bytes 163872 | tf_op jit(solution)/shard_map/ppermute | solution.py:367
  55.4 3.6 %collective-permute-start.4 = (bf16[80,1024]{1,0:T(8,128)(2,1)}, bf16[80,1024]{1,0:T(8,128)(2,1)S(1)}, u32[]{:S(2)}, u32[]{:S(2)}) collective-permute-start(bf16[80,1024]{1,0:T(8,128)(2,1)} %get-tuple-element.17), channel_id=1, source_target_pairs={{0,64},{32,96},{64,0},{96,32},{1,65},{33,97},{65,1},{97,33},{2,66}... | collective-permute-start | bytes 491528 | tf_op jit(solution)/shard_map/ppermute | solution.py:395
  60.0 8.1 %inside.1 = (f32[384,1024]{1,0:T(8,128)}, bf16[384,1024]{1,0:T(8,128)(2,1)}) custom-call(bf16[384,1024]{1,0:T(8,128)(2,1)} %bitcast.80, bf16[384,1024]{1,0:T(8,128)(2,1)} %bitcast.69, bf16[384,1024]{1,0:T(8,128)(2,1)} %bitcast.71, f32[1,1024]{1,0:T(1,128)} %bitcast.86, f32[384,16]{1,0:T(8,128)} %bitcast.76), custom_call_target="tpu_custom_call" | custom-call | tf_op jit(solution)/shard_map/inside/pallas_call | solution.py:369
  70.4 13.5 %mix.1 = (bf16[384,2048]{1,0:T(8,128)(2,1)S(1)}, bf16[768,2048]{1,0:T(8,128)(2,1)}, bf16[768,2048]{1,0:T(8,128)(2,1)}) custom-call(s32[3]{0:T(128)S(1)} %pad_add_fusion.pos_ref, f32[384,1024]{1,0:T(8,128)} %get-tuple-element.13.out_ref, bf16[384,1024]{1,0:T(8,128)(2,1)S(1)} %copy-done.4, bf16[384,1024]{1,0:T(8,128)(2,1)S(1)} %bitcast.58, ...), custom_call_target="tpu_custom_call" | custom-call | tf_op jit(solution)/shard_map/mix/pallas_call | solution.py:412
  83.9 43.6 %all_to_all.20 = bf16[16,48,2048]{2,1,0:T(8,128)(2,1)} all-to-all(bf16[16,48,2048]{2,1,0:T(8,128)(2,1)} %bitcast.65), channel_id=1, replica_groups=mesh['sp_0'=4,'sp_1'=4,'x'=4,'c'=2] {'sp_0','sp_1'}, dimensions={0} | all-to-all | bytes 6291456 | tf_op jit(solution)/shard_map/all_to_all | solution.py:453
  127.5 3.9 %all-to-all-start = ((bf16[16,48,2048]{2,1,0:T(8,128)(2,1)}), bf16[16,48,2048]{2,1,0:T(8,128)(2,1)S(1)}, u32[]{:S(2)}, u32[]{:S(2)}) async-start(bf16[16,48,2048]{2,1,0:T(8,128)(2,1)} %bitcast.19), calls=%async_computation | async-start | bytes 6291456 | tf_op jit(solution)/shard_map/all_to_all | solution.py:453
  131.4 6.6 %fusion.4 = f32[768,1024]{1,0:T(8,128)S(1)} fusion(bf16[768,2048]{1,0:T(8,128)(2,1)} %bitcast.66, bf16[1,2048,1024]{2,1,0:T(8,128)(2,1)} %param.24), kind=kOutput, calls=%fused_computation.4 | convolution fusion | flops 3221225472 | bytes 10485760 | tf_op jit(solution)/shard_map/dot_general | solution.py:459
  138.1 3.8 %multiply_convert_fusion = bf16[768,1024]{1,0:T(8,128)(2,1)S(1)} fusion(f32[768,1024]{1,0:T(8,128)S(1)} %fusion.4, bf16[768,2048]{1,0:T(8,128)(2,1)S(1)} %bitcast.67, bf16[1,2048,1024]{2,1,0:T(8,128)(2,1)S(1)} %copy-done.18), kind=kOutput, calls=%fused_computation.14 | convolution fusion | flops 3225944064 | bytes 12058624 | tf_op jit(solution)/shard_map/dot_general | solution.py:458
  141.9 4.8 %fusion.15 = bf16[768,2048]{1,0:T(8,128)(2,1)} fusion(bf16[768,1024]{1,0:T(8,128)(2,1)S(1)} %multiply_convert_fusion, bf16[1,1024,2048]{2,1,0:T(8,128)(2,1)S(1)} %copy-done.20), kind=kOutput, calls=%fused_computation.13 | convolution fusion | flops 3222798336 | bytes 8912896 | tf_op jit(solution)/shard_map/dot_general | solution.py:461
  146.8 27.6 %all-to-all-done = bf16[16,48,2048]{2,1,0:T(8,128)(2,1)S(1)} async-done(((bf16[16,48,2048]{2,1,0:T(8,128)(2,1)}), bf16[16,48,2048]{2,1,0:T(8,128)(2,1)S(1)}, u32[]{:S(2)}, u32[]{:S(2)}) %all-to-all-start) | async-done | bytes 3145760 | tf_op jit(solution)/shard_map/all_to_all | solution.py:453
  176.0 3.9 %all-to-all-start.3 = ((bf16[16,48,2048]{2,1,0:T(8,128)(2,1)}), bf16[16,48,2048]{2,1,0:T(8,128)(2,1)S(1)}, u32[]{:S(2)}, u32[]{:S(2)}) async-start(bf16[16,48,2048]{2,1,0:T(8,128)(2,1)} %bitcast.63), calls=%async_computation.3 | async-start | bytes 6291456 | tf_op jit(solution)/shard_map/all_to_all | solution.py:453
  179.9 6.6 %fusion.6 = f32[768,1024]{1,0:T(8,128)S(1)} fusion(bf16[768,2048]{1,0:T(8,128)(2,1)} %bitcast.61, bf16[1,2048,1024]{2,1,0:T(8,128)(2,1)} %param.24), kind=kOutput, calls=%fused_computation.6 | convolution fusion | flops 3221225472 | bytes 10485760 | tf_op jit(solution)/shard_map/dot_general | solution.py:459
  186.6 3.8 %multiply_convert_fusion.1 = bf16[768,1024]{1,0:T(8,128)(2,1)S(1)} fusion(f32[768,1024]{1,0:T(8,128)S(1)} %fusion.6, bf16[768,2048]{1,0:T(8,128)(2,1)S(1)} %bitcast.62, bf16[1,2048,1024]{2,1,0:T(8,128)(2,1)S(1)} %copy-done.19), kind=kOutput, calls=%fused_computation.15 | convolution fusion | flops 3225944064 | bytes 12058624 | tf_op jit(solution)/shard_map/dot_general | solution.py:458
  190.3 4.8 %fusion.12 = bf16[768,2048]{1,0:T(8,128)(2,1)} fusion(bf16[768,1024]{1,0:T(8,128)(2,1)S(1)} %multiply_convert_fusion.1, bf16[1,1024,2048]{2,1,0:T(8,128)(2,1)S(1)} %copy-done.21), kind=kOutput, calls=%fused_computation.12 | convolution fusion | flops 3222798336 | bytes 8912896 | tf_op jit(solution)/shard_map/dot_general | solution.py:461
  195.1 29.5 %all-to-all-done.3 = bf16[16,48,2048]{2,1,0:T(8,128)(2,1)S(1)} async-done(((bf16[16,48,2048]{2,1,0:T(8,128)(2,1)}), bf16[16,48,2048]{2,1,0:T(8,128)(2,1)S(1)}, u32[]{:S(2)}, u32[]{:S(2)}) %all-to-all-start.3) | async-done | bytes 3145760 | tf_op jit(solution)/shard_map/all_to_all | solution.py:453
  226.3 4.7 %all-to-all-start.1 = ((bf16[16,48,2048]{2,1,0:T(8,128)(2,1)}), bf16[16,48,2048]{2,1,0:T(8,128)(2,1)}, u32[]{:S(2)}, u32[]{:S(2)}) async-start(bf16[16,48,2048]{2,1,0:T(8,128)(2,1)} %bitcast.64), calls=%async_computation.1 | async-start | bytes 6291456 | tf_op jit(solution)/shard_map/all_to_all | solution.py:453
  231.9 7.3 %combine.2.acc_ref = f32[384,2048]{1,0:T(8,128)} custom-call(s32[384,2]{1,0:T(8,128)} %bitcast.73, f32[384,2]{1,0:T(8,128)} %bitcast.77, bf16[768,2048]{1,0:T(8,128)(2,1)} %bitcast.60, bf16[384,2048]{1,0:T(8,128)(2,1)} %copy-done.2), custom_call_target="tpu_custom_call" | custom-call | tf_op jit(solution)/shard_map/combine/pallas_call | solution.py:465
  239.2 33.2 %all-to-all-done.1 = bf16[16,48,2048]{2,1,0:T(8,128)(2,1)} async-done(((bf16[16,48,2048]{2,1,0:T(8,128)(2,1)}), bf16[16,48,2048]{2,1,0:T(8,128)(2,1)}, u32[]{:S(2)}, u32[]{:S(2)}) %all-to-all-start.1) | async-done | bytes 3145760 | tf_op jit(solution)/shard_map/all_to_all | solution.py:453
  272.3 7.3 %combine.3 = bf16[384,2048]{1,0:T(8,128)(2,1)} custom-call(s32[384,2]{1,0:T(8,128)} %bitcast.74, f32[384,2]{1,0:T(8,128)} %bitcast.78, bf16[768,2048]{1,0:T(8,128)(2,1)} %bitcast.25.got_ref, f32[384,2048]{1,0:T(8,128)} %combine.2.acc_ref), custom_call_target="tpu_custom_call" | custom-call | tf_op jit(solution)/shard_map/combine/pallas_call | solution.py:465
  (67 shorter events, 24.0 us)
Async XLA Ops:
  0.0 30.2 %copy-start = (f32[1,6144,16]{1,2,0:T(8,128)S(1)}, f32[1,6144,16]{1,2,0:T(8,128)}, u32[]{:S(2)}) copy-start(f32[1,6144,16]{1,2,0:T(8,128)} %param.19) | copy-start | bytes 1179652
  0.0 15.0 %collective-permute-start.6 = (bf16[128,2048]{1,0:T(8,128)(2,1)}, bf16[128,2048]{1,0:T(8,128)(2,1)S(1)}, u32[]{:S(2)}, u32[]{:S(2)}) collective-permute-start(bf16[128,2048]{1,0:T(8,128)(2,1)} %param.21), channel_id=1, source_target_pairs={{0,2},{2,4},{4,6},{6,0},{1,3},{3,5},{5,7},{7,1},{8,10},{10,12},{12... | collective-permute-start | bytes 1572872 | tf_op jit(solution)/shard_map/ppermute | solution.py:353
  1.6 25.8 %collective-permute-start.7 = (bf16[128,2048]{1,0:T(8,128)(2,1)}, bf16[128,2048]{1,0:T(8,128)(2,1)S(1)}, u32[]{:S(2)}, u32[]{:S(2)}) collective-permute-start(bf16[128,2048]{1,0:T(8,128)(2,1)} %param.21), channel_id=1, source_target_pairs={{0,4},{2,6},{4,0},{6,2},{1,5},{3,7},{5,1},{7,3},{8,12},{10,14},{12... | collective-permute-start | bytes 1572872 | tf_op jit(solution)/shard_map/ppermute | solution.py:353
  4.3 23.1 %collective-permute-start.8 = (bf16[128,2048]{1,0:T(8,128)(2,1)}, bf16[128,2048]{1,0:T(8,128)(2,1)S(1)}, u32[]{:S(2)}, u32[]{:S(2)}) collective-permute-start(bf16[128,2048]{1,0:T(8,128)(2,1)} %param.21), channel_id=1, source_target_pairs={{0,6},{2,0},{4,2},{6,4},{1,7},{3,1},{5,3},{7,5},{8,14},{10,8},{12,... | collective-permute-start | bytes 1572872 | tf_op jit(solution)/shard_map/ppermute | solution.py:353
  30.1 38.0 %copy-start.16 = (s32[1,384,2]{1,2,0:T(2,128)S(1)}, s32[1,384,2]{1,2,0:T(2,128)}, u32[]{:S(2)}) copy-start(s32[1,384,2]{1,2,0:T(2,128)} %param.26) | copy-start | bytes 9220
  30.1 38.4 %copy-start.3 = (bf16[1,384,1024]{2,1,0:T(8,128)(2,1)S(1)}, bf16[1,384,1024]{2,1,0:T(8,128)(2,1)}, u32[]{:S(2)}) copy-start(bf16[1,384,1024]{2,1,0:T(8,128)(2,1)} %param.17) | copy-start | bytes 2359300
  30.1 38.4 %copy-start.7 = (f32[2048]{0:T(1024)S(1)}, f32[2048]{0:T(1024)}, u32[]{:S(2)}) copy-start(f32[2048]{0:T(1024)} %param.22) | copy-start | bytes 24580
  30.1 38.4 %collective-permute-start.9 = (bf16[4,128,2048]{2,1,0:T(8,128)(2,1)}, bf16[4,128,2048]{2,1,0:T(8,128)(2,1)}, u32[]{:S(2)}, u32[]{:S(2)}) collective-permute-start(bf16[4,128,2048]{2,1,0:T(8,128)(2,1)} %pad_maximum_fusion.wmine_ref), channel_id=1, source_target_pairs={{0,1},{1,0},{2,3},{3,2},{4,5},{5,4},{6,7},{7,6},{8,9},{9,8},{10,11... | collective-permute-start | bytes 6291464 | tf_op jit(solution)/shard_map/ppermute | solution.py:398
  37.9 8.1 %collective-permute-start = (bf16[80,1024]{1,0:T(8,128)(2,1)}, bf16[80,1024]{1,0:T(8,128)(2,1)S(1)}, u32[]{:S(2)}, u32[]{:S(2)}) collective-permute-start(bf16[80,1024]{1,0:T(8,128)(2,1)} %states.1.own_ref), channel_id=1, source_target_pairs={{0,8},{8,16},{16,24},{24,0},{1,9},{9,17},{17,25},{25,1},{2,10},{10... | collective-permute-start | bytes 491528 | tf_op jit(solution)/shard_map/ppermute | solution.py:367
  39.5 11.2 %collective-permute-start.1 = (bf16[80,1024]{1,0:T(8,128)(2,1)}, bf16[80,1024]{1,0:T(8,128)(2,1)S(1)}, u32[]{:S(2)}, u32[]{:S(2)}) collective-permute-start(bf16[80,1024]{1,0:T(8,128)(2,1)} %states.1.own_ref), channel_id=1, source_target_pairs={{0,16},{8,24},{16,0},{24,8},{1,17},{9,25},{17,1},{25,9},{2,18},{10... | collective-permute-start | bytes 491528 | tf_op jit(solution)/shard_map/ppermute | solution.py:367
  42.4 8.3 %collective-permute-start.2 = (bf16[80,1024]{1,0:T(8,128)(2,1)}, bf16[80,1024]{1,0:T(8,128)(2,1)S(1)}, u32[]{:S(2)}, u32[]{:S(2)}) collective-permute-start(bf16[80,1024]{1,0:T(8,128)(2,1)} %states.1.own_ref), channel_id=1, source_target_pairs={{0,24},{8,0},{16,8},{24,16},{1,25},{9,1},{17,9},{25,17},{2,26},{10... | collective-permute-start | bytes 491528 | tf_op jit(solution)/shard_map/ppermute | solution.py:367
  53.5 15.0 %copy-start.5 = (f32[64,1024]{1,0:T(8,128)S(1)}, f32[64,1024]{1,0:T(8,128)}, u32[]{:S(2)}) copy-start(f32[64,1024]{1,0:T(8,128)} %get-tuple-element.15.before_ref) | copy-start | bytes 786436
  53.5 15.0 %collective-permute-start.3 = (bf16[80,1024]{1,0:T(8,128)(2,1)}, bf16[80,1024]{1,0:T(8,128)(2,1)S(1)}, u32[]{:S(2)}, u32[]{:S(2)}) collective-permute-start(bf16[80,1024]{1,0:T(8,128)(2,1)} %get-tuple-element.17), channel_id=1, source_target_pairs={{0,32},{32,64},{64,96},{96,0},{1,33},{33,65},{65,97},{97,1},{2,34}... | collective-permute-start | bytes 491528 | tf_op jit(solution)/shard_map/ppermute | solution.py:395
  55.4 13.0 %collective-permute-start.4 = (bf16[80,1024]{1,0:T(8,128)(2,1)}, bf16[80,1024]{1,0:T(8,128)(2,1)S(1)}, u32[]{:S(2)}, u32[]{:S(2)}) collective-permute-start(bf16[80,1024]{1,0:T(8,128)(2,1)} %get-tuple-element.17), channel_id=1, source_target_pairs={{0,64},{32,96},{64,0},{96,32},{1,65},{33,97},{65,1},{97,33},{2,66}... | collective-permute-start | bytes 491528 | tf_op jit(solution)/shard_map/ppermute | solution.py:395
  59.0 9.5 %collective-permute-start.5 = (bf16[80,1024]{1,0:T(8,128)(2,1)}, bf16[80,1024]{1,0:T(8,128)(2,1)S(1)}, u32[]{:S(2)}, u32[]{:S(2)}) collective-permute-start(bf16[80,1024]{1,0:T(8,128)(2,1)} %get-tuple-element.17), channel_id=1, source_target_pairs={{0,96},{32,0},{64,32},{96,64},{1,97},{33,1},{65,33},{97,65},{2,98}... | collective-permute-start | bytes 491528 | tf_op jit(solution)/shard_map/ppermute | solution.py:395
  68.3 15.7 %copy-start.12 = (s32[1,384,2]{2,1,0:T(8,128)}, s32[1,384,2]{2,1,0:T(8,128)S(1)}, u32[]{:S(2)}) copy-start(s32[1,384,2]{2,1,0:T(8,128)S(1)} %copy.15) | copy-start | bytes 9220
  83.9 43.6 %copy-start.2 = (bf16[384,2048]{1,0:T(8,128)(2,1)}, bf16[384,2048]{1,0:T(8,128)(2,1)S(1)}, u32[]{:S(2)}) copy-start(bf16[384,2048]{1,0:T(8,128)(2,1)S(1)} %get-tuple-element.20.acc_ref) | copy-start | bytes 4718596
  127.5 46.9 %all-to-all-start = ((bf16[16,48,2048]{2,1,0:T(8,128)(2,1)}), bf16[16,48,2048]{2,1,0:T(8,128)(2,1)S(1)}, u32[]{:S(2)}, u32[]{:S(2)}) async-start(bf16[16,48,2048]{2,1,0:T(8,128)(2,1)} %bitcast.19), calls=%async_computation | async-start | bytes 6291456 | tf_op jit(solution)/shard_map/all_to_all | solution.py:453
  131.4 6.7 %copy-start.11 = (bf16[16,48,2048]{2,1,0:T(8,128)(2,1)S(1)}, bf16[16,48,2048]{2,1,0:T(8,128)(2,1)}, u32[]{:S(2)}) copy-start(bf16[16,48,2048]{2,1,0:T(8,128)(2,1)} %all_to_all.20) | copy-start | bytes 9437188
  131.4 6.7 %copy-start.18 = (bf16[1,2048,1024]{2,1,0:T(8,128)(2,1)S(1)}, bf16[1,2048,1024]{2,1,0:T(8,128)(2,1)}, u32[]{:S(2)}) copy-start(bf16[1,2048,1024]{2,1,0:T(8,128)(2,1)} %param.23) | copy-start | bytes 12582916
  176.0 48.6 %all-to-all-start.3 = ((bf16[16,48,2048]{2,1,0:T(8,128)(2,1)}), bf16[16,48,2048]{2,1,0:T(8,128)(2,1)S(1)}, u32[]{:S(2)}, u32[]{:S(2)}) async-start(bf16[16,48,2048]{2,1,0:T(8,128)(2,1)} %bitcast.63), calls=%async_computation.3 | async-start | bytes 6291456 | tf_op jit(solution)/shard_map/all_to_all | solution.py:453
  179.9 6.7 %copy-start.10 = (bf16[16,48,2048]{2,1,0:T(8,128)(2,1)S(1)}, bf16[16,48,2048]{2,1,0:T(8,128)(2,1)}, u32[]{:S(2)}) copy-start(bf16[16,48,2048]{2,1,0:T(8,128)(2,1)} %copy-done.9) | copy-start | bytes 9437188
  226.3 46.0 %all-to-all-start.1 = ((bf16[16,48,2048]{2,1,0:T(8,128)(2,1)}), bf16[16,48,2048]{2,1,0:T(8,128)(2,1)}, u32[]{:S(2)}, u32[]{:S(2)}) async-start(bf16[16,48,2048]{2,1,0:T(8,128)(2,1)} %bitcast.64), calls=%async_computation.1 | async-start | bytes 6291456 | tf_op jit(solution)/shard_map/all_to_all | solution.py:453
  272.3 7.3 %copy-start.1 = (f32[1,6144,16]{1,2,0:T(8,128)S(1)}, f32[1,6144,16]{1,2,0:T(8,128)}, u32[]{:S(2)}) copy-start(f32[1,6144,16]{1,2,0:T(8,128)} %param.19) | copy-start | bytes 1179652
  (11 other events, 32.0 us)
where the time goes:
time: 280 us
  waiting for transfers between devices  119 us (42%)
  Pallas kernels  45.2 us (16%)
  blocking collectives  43.6 us (16%)
  starting transfers between devices  30.6 us (11%)
  matrix products  30.4 us (11%)
  local copies, waits for them, and re-layouts  7.91 us (3%)
    all_to_all x3, waiting for transfers between devices, exchange(): lax.all_to_all(a.reshape(experts, half, model), SP, split_axis=0, concat_...  90.3 us
    all_to_all x1, blocking collectives, exchange(): lax.all_to_all(a.reshape(experts, half, model), SP, split_axis=0, concat_...  43.6 us
    ppermute x3, waiting for transfers between devices, per_device(): lax.ppermute(output_weight, 'x', ring(n))  21.7 us
    pallas_call x2, Pallas kernels, combine(): pl.pallas_call(functools.partial(combine_kernel, cap, half, base, last),...  14.6 us
    pallas_call x1, Pallas kernels, per_device(): pl.pallas_call(functools.partial(mix_kernel, tok_steps, half), grid=(tok_...  13.5 us
    dot_general x2, matrix products, serve(): upward = jnp.dot(a, expert_up_weight[0], preferred_element_type=F32)  13.3 us
    all_to_all x3, starting transfers between devices, exchange(): lax.all_to_all(a.reshape(experts, half, model), SP, split_axis=0, concat_...  12.5 us
    dot_general x2, matrix products, serve(): jnp.dot(hidden, expert_down_weight[0], preferred_element_type=F32)  9.61 us
  transfers between devices with their start and end apart: 13, of which 7 were waited for; matrix products, arithmetic and copies ran while one was open for 12% of the time, Pallas kernels for 9%

commit v1 on v0

--- a/solution.py
+++ b/solution.py
@@ -58,13 +58,14 @@
     poly = jnp.full_like(keys, 1.0 / 10.0)
     for n in range(9, 0, -1):
         poly = poly * keys + 1.0 / n
-    heads = spike_ref.shape[1]
+    heads = spike_ref.shape[0]
     spread = (
         lax.broadcasted_iota(jnp.int32, (heads, GL), 0)
         == group * (GL // CH) + lax.broadcasted_iota(jnp.int32, (heads, GL), 1) // CH
     ).astype(BF)
     hi, mid, low = split3(spike_ref[...])
-    burst = dot(hi, spread) + dot(mid, spread) + dot(low, spread)
+    over = ((0,), (0,))
+    burst = dot(hi, spread, over) + dot(mid, spread, over) + dot(low, spread, over)
     return keys, burst - keys * poly
 
 
@@ -176,7 +177,7 @@
 
 def mix_kernel(
     tok_steps,
-    half,
+    cap,
     pos_ref,
     out_ref,
     qrun_ref,
@@ -187,19 +188,12 @@
     one_ref,
     two_ref,
     three_ref,
-    wmine_ref,
-    wother_ref,
-    scale_ref,
-    routes_ref,
-    upd_ref,
-    send_a_ref,
-    send_b_ref,
-    w_s,
-    state_s,
-    norm_s,
-    pos_s,
-    mem_s,
+    *refs,
 ):
+    wmine = refs[0:4]
+    wother = refs[4:8]
+    scale_ref, routes_ref, upd_ref, send_ref, w_s, state_s, norm_s, pos_s = refs[8:]
+
     step = pl.program_id(0)
     width = gate_ref.shape[1]
     groups = width // GL
@@ -221,12 +215,12 @@
             state_s[g] = jnp.where(mask, jnp.concatenate([one] * 4, axis=0), jnp.zeros((GL, GL), BF))
         x_here = pos_ref[1]
         core = pos_ref[2]
-        piece = wmine_ref.shape[1]
+        piece = wmine[0].shape[0]
         for n in range(4):
             src = (x_here + 4 - n) % 4
-            w_s[pl.ds((2 * src + core) * piece, piece), :] = wmine_ref[n]
-            w_s[pl.ds((2 * src + 1 - core) * piece, piece), :] = wother_ref[n]
-        experts = mem_s.shape[0]
+            w_s[pl.ds((2 * src + core) * piece, piece), :] = wmine[n][...]
+            w_s[pl.ds((2 * src + 1 - core) * piece, piece), :] = wother[n][...]
+        experts = pos_s.shape[0]
         e = lax.broadcasted_iota(jnp.int32, (experts, tok_rows), 0)
         member = (e == routes_ref[0:1, :]) | (e == routes_ref[1:2, :])
         mem = jnp.where(member, 1.0, 0.0)
@@ -256,56 +250,65 @@
         norm = (wide * lax.rsqrt(mean + 1e-06) * scale_ref[...]).astype(BF)
         norm_s[pl.ds(step * rows, rows), :] = norm
 
-    def send(ref, first, base):
+    @pl.when(step >= tok_steps)
+    def _():
+        per = send_ref.shape[0] // cap
         picks = []
-        for i in range(ref.shape[0] // half):
-            place = pos_s[pl.ds(first + i, 1), :]
-            c = lax.broadcasted_iota(jnp.int32, (half, tok_rows), 0) + base
+        for i in range(per):
+            place = pos_s[pl.ds((step - tok_steps) * per + i, 1), :]
+            c = lax.broadcasted_iota(jnp.int32, (cap, tok_rows), 0)
             picks.append(jnp.where(c == place, 1.0, 0.0).astype(BF))
-        ref[...] = dot(jnp.concatenate(picks, axis=0), norm_s[...]).astype(BF)
-
-    per = send_a_ref.shape[0] // half
-    blocks = mem_s.shape[0] // per
-
-    @pl.when((step >= tok_steps) & (step < tok_steps + blocks))
+        send_ref[...] = dot(jnp.concatenate(picks, axis=0), norm_s[...]).astype(BF)
+
+
+def serve_kernel(hid_steps, x_ref, wg_ref, wu_ref, wd_ref, out_ref, hid_s):
+    step = pl.program_id(1)
+    blk = wg_ref.shape[2]
+
+    for n in range(hid_steps):
+
+        @pl.when(step == n)
+        def _(n=n):
+            x = x_ref[...].reshape(hid_s.shape[0], x_ref.shape[2])
+            hidden = silu(dot(x, wg_ref[0])) * dot(x, wu_ref[0])
+            hid_s[:, n * blk : (n + 1) * blk] = hidden.astype(BF)
+
+    @pl.when(step >= hid_steps)
     def _():
-        send(send_a_ref, (step - tok_steps) * per, 0)
-
-    @pl.when(step >= tok_steps + blocks)
-    def _():
-        send(send_b_ref, (step - tok_steps - blocks) * per, half)
-
-
-def combine_kernel(cap, half, base, last, routes_ref, wt_ref, got_ref, acc_ref, out_ref, hi_s, low_s):
-    experts = got_ref.shape[0] // half
-    tok_rows = routes_ref.shape[0]
-
-    @pl.when(pl.program_id(0) == 0)
-    def _():
-        lane = lax.broadcasted_iota(jnp.int32, (tok_rows, 128), 1)
-        r0 = routes_ref[:, 0:1]
-        r1 = routes_ref[:, 1:2]
-        oh0 = lane == r0
-        oh1 = lane == r1
-        mem = jnp.where(oh0 | oh1, 1.0, 0.0).astype(BF)
-        strict = (
-            lax.broadcasted_iota(jnp.int32, (tok_rows, tok_rows), 0)
-            > lax.broadcasted_iota(jnp.int32, (tok_rows, tok_rows), 1)
-        ).astype(BF)
-        place = dot(strict, mem)
-        j = lax.broadcasted_iota(jnp.int32, (tok_rows, experts * half), 1)
-        weight = jnp.zeros((tok_rows, experts * half), F32)
-        for k, (oh, r) in enumerate(((oh0, r0), (oh1, r1))):
-            p = jnp.sum(jnp.where(oh, place, 0.0), axis=1, keepdims=True).astype(jnp.int32) - base
-            slot = jnp.where((p >= 0) & (p < half), r * half + p, -1)
-            weight = weight + jnp.where(j == slot, wt_ref[:, k : k + 1], 0.0)
-        hi, low = split2(weight)
-        hi_s[...] = hi
-        low_s[...] = low
-
-    got = got_ref[...]
-    total = acc_ref[...].astype(F32) + (dot(hi_s[...], got) + dot(low_s[...], got))
-    out_ref[...] = total.astype(out_ref.dtype)
+        out_ref[...] = dot(hid_s[...], wd_ref[0]).astype(BF).reshape(out_ref.shape)
+
+
+def weights_kernel(main, routes_ref, wt_ref, main_ref, rest_ref):
+    tok_rows = routes_ref.shape[1]
+    experts = main_ref.shape[1] // main
+    routes = jnp.transpose(routes_ref[...])
+    wts = jnp.transpose(wt_ref[...])
+    lane = lax.broadcasted_iota(jnp.int32, (tok_rows, 128), 1)
+    strict = (
+        lax.broadcasted_iota(jnp.int32, (tok_rows, tok_rows), 0)
+        > lax.broadcasted_iota(jnp.int32, (tok_rows, tok_rows), 1)
+    ).astype(BF)
+    ones = [lane == routes[:, k : k + 1] for k in range(2)]
+    place = dot(strict, jnp.where(ones[0] | ones[1], 1.0, 0.0).astype(BF))
+    for ref, base in ((main_ref, 0), (rest_ref, main)):
+        size = ref.shape[1] // experts
+        j = lax.broadcasted_iota(jnp.int32, ref.shape, 1)
+        weight = jnp.zeros(ref.shape, F32)
+        for k in range(2):
+            p = jnp.sum(jnp.where(ones[k], place, 0.0), axis=1, keepdims=True).astype(jnp.int32)
+            p = p - base
+            slot = jnp.where((p >= 0) & (p < size), routes[:, k : k + 1] * size + p, -1)
+            weight = jnp.where(j == slot, wts[:, k : k + 1], weight)
+        ref[...] = weight.astype(BF)
+
+
+def combine_kernel(main_ref, rest_ref, got_ref, got_rest_ref, upd_ref, out_ref):
+    total = dot(main_ref[...], got_ref[...]) + dot(rest_ref[...], got_rest_ref[...])
+    out_ref[...] = (upd_ref[...].astype(F32) + total).astype(out_ref.dtype)
+
+
+def cost(us):
+    return pl.CostEstimate(flops=int(us * 5e8), bytes_accessed=int(us * 1e6), transcendentals=0)
 
 
 def ring(n, size=4):
@@ -330,18 +333,18 @@
 ):
     _, tok, width = query_weight.shape
     model = output_weight.shape[1]
-    piece = output_weight.shape[0]
     heads = width // CH
     groups = width // GL
     experts = lax.axis_size(SP)
     cap = 4 * tok // experts
-    half = cap // 2
+    main = cap * 5 // 6
+    rest = cap - main
     z = lax.axis_index("sp_0")
     y = lax.axis_index("sp_1")
     x = lax.axis_index("x")
     core = lax.axis_index("c")
 
-    spikes = lax.dynamic_slice_in_dim(extra_log_decay[0], lax.axis_index(SP) * tok, tok, 0)
+    spikes = lax.dynamic_slice_in_dim(extra_log_decay[0].T, lax.axis_index(SP) * tok, tok, 1)
     q, f, v, gate = (
         a.reshape(tok, width)
         for a in (query_weight, forget_preactivation, written_input, output_gate_logit)
@@ -350,33 +353,24 @@
     scale = norm_scale_vector.reshape(1, model)
     res = residual.reshape(tok, model)
 
-    wpieces = [output_weight] + [lax.ppermute(output_weight, "x", ring(n)) for n in (1, 2, 3)]
+    mine = output_weight
+    wmine = [lax.ppermute(mine, "x", ring(n)) for n in (1, 2, 3)]
 
     tall = pl.BlockSpec((tok, GL), lambda g: (0, g))
     flat = pl.BlockSpec((1, GL), lambda g: (0, g))
-    whole = pl.BlockSpec((tok, heads), lambda g: (0, 0))
+    whole = pl.BlockSpec((heads, tok), lambda g: (0, 0))
     pack = pl.pallas_call(
         states_kernel,
         grid=(groups,),
         in_specs=[tall, tall, flat, whole],
         out_specs=pl.BlockSpec((PACK, GL), lambda g: (0, g)),
         out_shape=jax.ShapeDtypeStruct((PACK, width), BF),
+        cost_estimate=cost(7),
         name="states",
     )(f, v, floor, spikes)
 
     along_y = [lax.ppermute(pack, "sp_1", ring(n)) for n in (1, 2, 3)]
 
-    inside, qrun = pl.pallas_call(
-        inside_kernel,
-        grid=(groups,),
-        in_specs=[tall, tall, tall, flat, whole],
-        out_specs=[tall, tall],
-        out_shape=[
-            jax.ShapeDtypeStruct((tok, width), F32),
-            jax.ShapeDtypeStruct((tok, width), BF),
-        ],
-        name="inside",
-    )(q, f, v, floor, spikes)
 
     vm = pl.BlockSpec(memory_space=pltpu.VMEM)
     sm = pl.BlockSpec(memory_space=pltpu.SMEM)
@@ -389,28 +383,42 @@
             jax.ShapeDtypeStruct((CH, width), F32),
             jax.ShapeDtypeStruct((8, width), F32),
         ],
+        cost_estimate=cost(2),
         name="row",
     )(y.astype(jnp.int32).reshape(1), pack, *along_y)
 
     along_z = [lax.ppermute(row, "sp_0", ring(n)) for n in (1, 2, 3)]
 
-    wmine = jnp.stack(wpieces)
-    wother = lax.ppermute(wmine, "c", [(0, 1), (1, 0)])
+    q, row = lax.optimization_barrier((q, row))
+    inside, qrun = pl.pallas_call(
+        inside_kernel,
+        grid=(groups,),
+        in_specs=[tall, tall, tall, flat, whole],
+        out_specs=[tall, tall],
+        out_shape=[jax.ShapeDtypeStruct((tok, width), F32), jax.ShapeDtypeStruct((tok, width), BF)],
+        cost_estimate=cost(8),
+        name="inside",
+    )(q, f, v, floor, spikes)
+
+    wmine, qrun = lax.optimization_barrier((wmine, qrun))
+    wmine = [mine] + wmine
+    wother = [lax.ppermute(p, "c", ring(1, 2)) for p in wmine]
+
 
     route_rows = jnp.pad(routes[0].T, ((0, 6), (0, 0)), constant_values=-1)
     place = jnp.stack([z, x, core]).astype(jnp.int32)
     tok_steps = 3
     rows = tok // tok_steps
     send_steps = 4
-    send_rows = 2 * experts * half // send_steps
+    send_rows = experts * cap // send_steps
     clip = lambda i: jnp.minimum(i, tok_steps - 1)
     tok_w = pl.BlockSpec((rows, width), lambda i: (clip(i), 0))
     tok_m = pl.BlockSpec((rows, model), lambda i: (clip(i), 0))
     full = lambda a: pl.BlockSpec(a.shape, lambda i: (0,) * a.ndim)
 
 
-    updated, send_a, send_b = pl.pallas_call(
-        functools.partial(mix_kernel, tok_steps, half),
+    updated, send = pl.pallas_call(
+        functools.partial(mix_kernel, tok_steps, cap),
         grid=(tok_steps + send_steps,),
         in_specs=[
             sm,
@@ -423,66 +431,104 @@
             full(row),
             full(row),
             full(row),
-            full(wmine),
-            full(wmine),
+            *[full(mine)] * 8,
             full(scale),
             full(route_rows),
         ],
         out_specs=[
             tok_m,
-            pl.BlockSpec((send_rows, model), lambda i: (jnp.clip(i - tok_steps, 0, 1), 0)),
-            pl.BlockSpec((send_rows, model), lambda i: (jnp.clip(i - tok_steps - 2, 0, 1), 0)),
+            pl.BlockSpec((send_rows, model), lambda i: (jnp.maximum(i - tok_steps, 0), 0)),
         ],
         out_shape=[
             jax.ShapeDtypeStruct((tok, model), BF),
-            jax.ShapeDtypeStruct((experts * half, model), BF),
-            jax.ShapeDtypeStruct((experts * half, model), BF),
+            jax.ShapeDtypeStruct((experts * cap, model), BF),
         ],
         scratch_shapes=[
             pltpu.VMEM((width, model), BF),
             pltpu.VMEM((groups, GL, GL), BF),
             pltpu.VMEM((tok, model), BF),
             pltpu.VMEM((experts, tok), jnp.int32),
-            pltpu.VMEM((experts, tok), jnp.int32),
         ],
         compiler_params=pltpu.CompilerParams(vmem_limit_bytes=50 * 1024 * 1024),
+        cost_estimate=cost(12),
         name="mix",
-    )(place, inside, qrun, gate, res, before, btot, *along_z, wmine, wother, scale, route_rows)
+    )(place, inside, qrun, gate, res, before, btot, *along_z, *wmine, *wother, scale, route_rows)
 
     def exchange(a):
-        return lax.all_to_all(
-            a.reshape(experts, half, model), SP, split_axis=0, concat_axis=0, tiled=True
-        ).reshape(experts * half, model)
-
-    def serve(a):
-        gated = jnp.dot(a, expert_gate_weight[0], preferred_element_type=F32)
-        upward = jnp.dot(a, expert_up_weight[0], preferred_element_type=F32)
-        hidden = (jax.nn.silu(gated) * upward).astype(BF)
-        return jnp.dot(hidden, expert_down_weight[0], preferred_element_type=F32).astype(BF)
-
-    def combine(got, acc, base, last):
-        blk = 512
+        return lax.all_to_all(a, SP, split_axis=0, concat_axis=0, tiled=True)
+
+    hid = expert_gate_weight.shape[2]
+    hid_steps = 2
+    out_steps = 2
+
+    def serve(arrived, first, size, blocks):
+        srcs = experts // blocks
+        where = first // size
+        up = pl.BlockSpec(
+            (1, model, hid // hid_steps), lambda m, j: (0, 0, jnp.minimum(j, hid_steps - 1))
+        )
+        after = lambda j: jnp.maximum(j - hid_steps, 0)
         return pl.pallas_call(
-            functools.partial(combine_kernel, cap, half, base, last),
-            grid=(model // blk,),
+            functools.partial(serve_kernel, hid_steps),
+            grid=(blocks, hid_steps + out_steps),
             in_specs=[
-                pl.BlockSpec((tok, 2), lambda i: (0, 0)),
-                pl.BlockSpec((tok, 2), lambda i: (0, 0)),
-                pl.BlockSpec((experts * half, blk), lambda i: (0, i)),
-                pl.BlockSpec((tok, blk), lambda i: (0, i)),
+                pl.BlockSpec((srcs, size, model), lambda m, j: (m, where, 0)),
+                up,
+                up,
+                pl.BlockSpec((1, hid, model // out_steps), lambda m, j: (0, 0, after(j))),
             ],
-            out_specs=pl.BlockSpec((tok, blk), lambda i: (0, i)),
-            out_shape=jax.ShapeDtypeStruct((tok, model), BF if last else F32),
-            scratch_shapes=[pltpu.VMEM((tok, experts * half), BF)] * 2,
-            name="combine",
-        )(routes[0], routing_weight[0], got, acc)
-
-    in_a = exchange(send_a)
-    in_b = exchange(send_b)
-    got_a = exchange(serve(in_a))
-    got_b = exchange(serve(in_b))
-    acc = combine(got_a, updated, 0, False)
-    layer_out = combine(got_b, acc, half, True)
+            out_specs=pl.BlockSpec((srcs, size, model // out_steps), lambda m, j: (m, 0, after(j))),
+            out_shape=jax.ShapeDtypeStruct((experts, size, model), BF),
+            scratch_shapes=[pltpu.VMEM((srcs * size, hid), BF)],
+            compiler_params=pltpu.CompilerParams(vmem_limit_bytes=50 * 1024 * 1024),
+            cost_estimate=cost(18 if blocks > 1 else 5),
+            name="serve",
+        )(arrived, expert_gate_weight, expert_up_weight, expert_down_weight)
+
+    arrived = exchange(send.reshape(experts, cap, model))
+    served_rest = serve(arrived, main, rest, 1)
+    got_rest = exchange(served_rest)
+
+    picks, _ = lax.optimization_barrier((route_rows, served_rest))
+    weights_main, weights_rest = pl.pallas_call(
+        functools.partial(weights_kernel, main),
+        in_specs=[vm, vm],
+        out_specs=[vm, vm],
+        out_shape=[
+            jax.ShapeDtypeStruct((tok, experts * main), BF),
+            jax.ShapeDtypeStruct((tok, experts * rest), BF),
+        ],
+        cost_estimate=cost(2),
+        name="weights",
+    )(picks, jnp.pad(routing_weight[0].T, ((0, 6), (0, 0))))
+    arrived, weights_main, weights_rest = lax.optimization_barrier(
+        (arrived, weights_main, weights_rest)
+    )
+    got = exchange(serve(arrived, 0, main, 2))
+
+    blk = 512
+    col = lambda r: pl.BlockSpec((r, blk), lambda i: (0, i))
+    layer_out = pl.pallas_call(
+        combine_kernel,
+        grid=(model // blk,),
+        in_specs=[
+            full(weights_main),
+            full(weights_rest),
+            col(experts * main),
+            col(experts * rest),
+            col(tok),
+        ],
+        out_specs=col(tok),
+        out_shape=jax.ShapeDtypeStruct((tok, model), BF),
+        cost_estimate=cost(4),
+        name="combine",
+    )(
+        weights_main,
+        weights_rest,
+        got.reshape(experts * main, model),
+        got_rest.reshape(experts * rest, model),
+        updated,
+    )
     return layer_out.reshape(1, tok, model)
 
 

time: 280 us -> 276 us (0.986)
  blocking collectives: 43.6 us -> 143 us
  waiting for transfers between devices: 119 us -> 27.5 us
  matrix products: 30.4 us -> 0 us
  Pallas kernels: 45.2 us -> 74.6 us
  starting transfers between devices: 30.6 us -> 21.4 us
    all_to_all x1 -> x2, blocking collectives: 43.6 us -> 143 us  [exchange(): return lax.all_to_all(a, SP, split_axis=0, concat_axis=0, tiled=True)]
    all_to_all x3 -> x1, waiting for transfers between devices: 90.3 us -> 0.01 us  [exchange(): return lax.all_to_all(a, SP, split_axis=0, concat_axis=0, tiled=True)]
    dot_general x6 -> x0, matrix products: 30.4 us -> none  [the longest x2 13.3 us: serve(): upward = jnp.dot(a, expert_up_weight[0], preferred_element_type=F32)]
    pallas_call x3 -> x5, Pallas kernels: 28.1 us -> 57.4 us  [the longest x2 34.8 us: serve(): pl.pallas_call(functools.partial(serve_kernel, hid_steps), grid=(blocks,...]
    ppermute x3, waiting for transfers between devices: 0.01 us -> 15.6 us  [per_device(): along_z = [lax.ppermute(row, 'sp_0', ring(n)) for n in (1, 2, 3)]]
    ppermute x4 -> x7, waiting for transfers between devices: 21.7 us -> 7.72 us  [the longest x3 7.71 us: per_device(): wmine = [lax.ppermute(mine, 'x', ring(n)) for n in (1, 2, 3)]]
    all_to_all x3 -> x1, starting transfers between devices: 12.5 us -> 3.66 us  [exchange(): return lax.all_to_all(a, SP, split_axis=0, concat_axis=0, tiled=True)]
    ppermute x4 -> x7, starting transfers between devices: 5.77 us -> 5.58 us  [the longest x3 5.05 us: per_device(): wmine = [lax.ppermute(mine, 'x', ring(n)) for n in (1, 2, 3)]]
  transfers between devices with their start and end apart: 13 -> 14, of which waited for: 7 -> 8; matrix products, arithmetic and copies ran while one was open for 12% -> 0% of each run, Pallas kernels for 9% -> 14%
where the time goes in v1:
time: 276 us; the launch traced here: 275 us
  blocking collectives  143 us (52%)
  Pallas kernels  74.6 us (27%)
  waiting for transfers between devices  27.5 us (10%)
  starting transfers between devices  21.4 us (8%)
  local copies, waits for them, and re-layouts  8.46 us (3%)
    all_to_all x2, blocking collectives, exchange(): return lax.all_to_all(a, SP, split_axis=0, concat_axis=0, tiled=True)  143 us
    pallas_call x2, Pallas kernels, serve(): pl.pallas_call(functools.partial(serve_kernel, hid_steps), grid=(blocks,...  34.8 us
    ppermute x3, waiting for transfers between devices, per_device(): along_z = [lax.ppermute(row, 'sp_0', ring(n)) for n in (1, 2, 3)]  15.6 us
    pallas_call x1, Pallas kernels, per_device(): pl.pallas_call(functools.partial(mix_kernel, tok_steps, cap), grid=(tok_s...  12.6 us
    pallas_call x1, Pallas kernels, per_device(): pl.pallas_call(inside_kernel, grid=(groups,), in_specs=[tall, tall, tall,...  8.26 us
    ppermute x3, waiting for transfers between devices, per_device(): wmine = [lax.ppermute(mine, 'x', ring(n)) for n in (1, 2, 3)]  7.71 us
    ppermute x3, starting transfers between devices, per_device(): along_z = [lax.ppermute(row, 'sp_0', ring(n)) for n in (1, 2, 3)]  7.45 us
    unnamed x32, local copies, waits for them, and re-layouts  7.25 us
  transfers between devices with their start and end apart: 14, of which 8 were waited for; matrix products, arithmetic and copies ran while one was open for 0% of the time, Pallas kernels for 14%

profile of v1, /device:TPU:0, one launch (start us, length us, event | category | flops | bytes accessed | tf_op | source)
XLA Modules:
  0.0 275.2 jit_solution(349687938732634886)
XLA Ops:
  1.6 6.8 %states.1.own_ref = bf16[80,1024]{1,0:T(8,128)(2,1)} custom-call(bf16[384,1024]{1,0:T(8,128)(2,1)} %bitcast.33, bf16[384,1024]{1,0:T(8,128)(2,1)} %bitcast.35, f32[1,1024]{1,0:T(1,128)} %bitcast.38, f32[16,384]{1,0:T(8,128)} %dynamic-slice_bitcast_fusion.spike_ref), custom_call_target="tpu_custom_call" | custom-call | flops 3500000000 | bytes 7000000 | tf_op jit(solution)/shard_map/states/pallas_call | solution.py:362
  8.4 3.1 %collective-permute-start.2 = (bf16[80,1024]{1,0:T(8,128)(2,1)}, bf16[80,1024]{1,0:T(8,128)(2,1)S(1)}, u32[]{:S(2)}, u32[]{:S(2)}) collective-permute-start(bf16[80,1024]{1,0:T(8,128)(2,1)} %states.1.own_ref), channel_id=1, source_target_pairs={{0,24},{8,0},{16,8},{24,16},{1,25},{9,1},{17,9},{25,17},{2,26},{10... | collective-permute-start | bytes 491528 | tf_op jit(solution)/shard_map/ppermute | solution.py:372
  13.2 2.8 %collective-permute-start.5 = (bf16[128,2048]{1,0:T(8,128)(2,1)S(1)}, bf16[128,2048]{1,0:T(8,128)(2,1)S(1)}, u32[]{:S(2)}, u32[]{:S(2)}) collective-permute-start(bf16[128,2048]{1,0:T(8,128)(2,1)S(1)} %copy-done.2), channel_id=1, source_target_pairs={{0,6},{2,0},{4,2},{6,4},{1,7},{3,1},{5,3},{7,5},{8,14},{10,8},{12,... | collective-permute-start | bytes 1572872 | tf_op jit(solution)/shard_map/ppermute | solution.py:357
  16.7 2.1 collective-permute-done.2.three_ref
  18.8 1.5 collective-permute-start.3
  20.4 2.0 collective-permute-done.one_ref
  23.1 2.1 row.1
  25.2 8.3 %inside.1 = (f32[384,1024]{1,0:T(8,128)}, bf16[384,1024]{1,0:T(8,128)(2,1)}) custom-call(bf16[384,1024]{1,0:T(8,128)(2,1)} %bitcast.32, bf16[384,1024]{1,0:T(8,128)(2,1)} %bitcast.34, bf16[384,1024]{1,0:T(8,128)(2,1)} %bitcast.36, f32[1,1024]{1,0:T(1,128)} %bitcast.39, f32[16,384]{1,0:T(8,128)} %dynamic-slice_bitcast_fusion.spike_ref), custom_call_target="tpu_custom_call" | custom-call | flops 4000000000 | bytes 8000000 | tf_op jit(solution)/shard_map/inside/pallas_call | solution.py:393
  33.5 4.0 %collective-permute-done.5.refs_3_ = bf16[128,2048]{1,0:T(8,128)(2,1)S(1)} collective-permute-done((bf16[128,2048]{1,0:T(8,128)(2,1)S(1)}, bf16[128,2048]{1,0:T(8,128)(2,1)S(1)}, u32[]{:S(2)}, u32[]{:S(2)}) %collective-permute-start.5) | collective-permute-done | bytes 524320 | tf_op jit(solution)/shard_map/ppermute | solution.py:357
  37.5 3.7 %collective-permute-done.3.refs_1_ = bf16[128,2048]{1,0:T(8,128)(2,1)S(1)} collective-permute-done((bf16[128,2048]{1,0:T(8,128)(2,1)S(1)}, bf16[128,2048]{1,0:T(8,128)(2,1)S(1)}, u32[]{:S(2)}, u32[]{:S(2)}) %collective-permute-start.3) | collective-permute-done | bytes 524320 | tf_op jit(solution)/shard_map/ppermute | solution.py:357
  41.7 4.0 %collective-permute-start.8 = (bf16[80,1024]{1,0:T(8,128)(2,1)}, bf16[80,1024]{1,0:T(8,128)(2,1)S(1)}, u32[]{:S(2)}, u32[]{:S(2)}) collective-permute-start(bf16[80,1024]{1,0:T(8,128)(2,1)} %get-tuple-element.23), channel_id=1, source_target_pairs={{0,96},{32,0},{64,32},{96,64},{1,97},{33,1},{65,33},{97,65},{2,98}... | collective-permute-start | bytes 491528 | tf_op jit(solution)/shard_map/ppermute | solution.py:390
  45.8 4.4 %collective-permute-done.8.three_ref = bf16[80,1024]{1,0:T(8,128)(2,1)S(1)} collective-permute-done((bf16[80,1024]{1,0:T(8,128)(2,1)}, bf16[80,1024]{1,0:T(8,128)(2,1)S(1)}, u32[]{:S(2)}, u32[]{:S(2)}) %collective-permute-start.8) | collective-permute-done | bytes 163872 | tf_op jit(solution)/shard_map/ppermute | solution.py:390
  50.9 2.2 collective-permute-start.7
  53.1 5.2 %collective-permute-done.7.two_ref = bf16[80,1024]{1,0:T(8,128)(2,1)S(1)} collective-permute-done((bf16[80,1024]{1,0:T(8,128)(2,1)}, bf16[80,1024]{1,0:T(8,128)(2,1)S(1)}, u32[]{:S(2)}, u32[]{:S(2)}) %collective-permute-start.7) | collective-permute-done | bytes 163872 | tf_op jit(solution)/shard_map/ppermute | solution.py:390
  59.0 1.2 collective-permute-start.6
  60.3 5.9 %collective-permute-done.6.one_ref = bf16[80,1024]{1,0:T(8,128)(2,1)} collective-permute-done((bf16[80,1024]{1,0:T(8,128)(2,1)}, bf16[80,1024]{1,0:T(8,128)(2,1)}, u32[]{:S(2)}, u32[]{:S(2)}) %collective-permute-start.6) | collective-permute-done | bytes 163872 | tf_op jit(solution)/shard_map/ppermute | solution.py:390
  70.5 12.6 %mix.1 = (bf16[384,2048]{1,0:T(8,128)(2,1)}, bf16[1536,2048]{1,0:T(8,128)(2,1)}) custom-call(s32[3]{0:T(128)S(1)} %pad_add_fusion.pos_ref, f32[384,1024]{1,0:T(8,128)} %get-tuple-element.25.out_ref, bf16[384,1024]{1,0:T(8,128)(2,1)} %get-tuple-element.27.qrun_ref, bf16[384,1024]{1,0:T(8,128)(2,1)} %bitcast.37, bf16[384,2048]{1,0:T(8,128)(2,1)} %bitcast.31, ...), custom_call_target="tpu_custom_call" | custom-call | flops 6000000000 | bytes 12000000 | tf_op jit(solution)/shard_map/mix/pallas_call | solution.py:420
  83.0 76.9 %all_to_all.15.x_ref = bf16[16,96,2048]{2,1,0:T(8,128)(2,1)} all-to-all(bf16[16,96,2048]{2,1,0:T(8,128)(2,1)} %bitcast.27), channel_id=1, replica_groups=mesh['sp_0'=4,'sp_1'=4,'x'=4,'c'=2] {'sp_0','sp_1'}, dimensions={0} | all-to-all | bytes 12582912 | tf_op jit(solution)/shard_map/all_to_all | solution.py:458
  159.9 8.8 %serve.2 = bf16[16,16,2048]{2,1,0:T(8,128)(2,1)} custom-call(bf16[16,96,2048]{2,1,0:T(8,128)(2,1)} %all_to_all.15.x_ref, bf16[1,2048,1024]{2,1,0:T(8,128)(2,1)} %wg_ref.3, bf16[1,2048,1024]{2,1,0:T(8,128)(2,1)} %wu_ref.3, bf16[1,1024,2048]{2,1,0:T(8,128)(2,1)} %wd_ref.3), custom_call_target="tpu_custom_call" | custom-call | flops 2500000000 | bytes 5000000 | tf_op jit(solution)/shard_map/serve/pallas_call | solution.py:471
  168.7 3.7 %all-to-all-start.2 = ((bf16[16,16,2048]{2,1,0:T(8,128)(2,1)}), bf16[16,16,2048]{2,1,0:T(8,128)(2,1)S(1)}, u32[]{:S(2)}, u32[]{:S(2)}) async-start(bf16[16,16,2048]{2,1,0:T(8,128)(2,1)} %serve.2), calls=%async_computation.2 | async-start | bytes 2097152 | tf_op jit(solution)/shard_map/all_to_all | solution.py:458
  173.0 3.2 %weights.1 = (bf16[384,1280]{1,0:T(8,128)(2,1)}, bf16[384,256]{1,0:T(8,128)(2,1)}) custom-call(s32[8,384]{1,0:T(8,128)} %copy-done.1, f32[8,384]{1,0:T(8,128)} %pad.9.wt_ref), custom_call_target="tpu_custom_call" | custom-call | flops 1000000000 | bytes 2000000 | tf_op jit(solution)/shard_map/weights/pallas_call | solution.py:493
  176.2 25.9 %serve.3 = bf16[16,80,2048]{2,1,0:T(8,128)(2,1)} custom-call(bf16[16,96,2048]{2,1,0:T(8,128)(2,1)} %all_to_all.15.x_ref, bf16[1,2048,1024]{2,1,0:T(8,128)(2,1)} %wg_ref.3, bf16[1,2048,1024]{2,1,0:T(8,128)(2,1)} %wu_ref.3, bf16[1,1024,2048]{2,1,0:T(8,128)(2,1)} %wd_ref.3), custom_call_target="tpu_custom_call" | custom-call | flops 8999999488 | bytes 18000000 | tf_op jit(solution)/shard_map/serve/pallas_call | solution.py:471
  202.1 66.2 %all_to_all.16 = bf16[16,80,2048]{2,1,0:T(8,128)(2,1)} all-to-all(bf16[16,80,2048]{2,1,0:T(8,128)(2,1)} %serve.3), channel_id=1, replica_groups=mesh['sp_0'=4,'sp_1'=4,'x'=4,'c'=2] {'sp_0','sp_1'}, dimensions={0} | all-to-all | bytes 10485760 | tf_op jit(solution)/shard_map/all_to_all | solution.py:458
  268.3 6.9 %combine.1 = bf16[384,2048]{1,0:T(8,128)(2,1)} custom-call(bf16[384,1280]{1,0:T(8,128)(2,1)} %get-tuple-element.37.main_ref, bf16[384,256]{1,0:T(8,128)(2,1)} %get-tuple-element.38.rest_ref, bf16[1280,2048]{1,0:T(8,128)(2,1)} %bitcast.26, bf16[256,2048]{1,0:T(8,128)(2,1)} %bitcast.28, bf16[384,2048]{1,0:T(8,128)(2,1)} %get-tuple-element.40.upd_ref), custom_call_target="tpu_custom_call" | custom-call | flops 2000000000 | bytes 4000000 | tf_op jit(solution)/shard_map/combine/pallas_call | solution.py:511
  (50 shorter events, 11.5 us)
Async XLA Ops:
  0.0 1.0 copy-start
  1.6 11.6 %copy-start.2 = (bf16[128,2048]{1,0:T(8,128)(2,1)S(1)}, bf16[128,2048]{1,0:T(8,128)(2,1)}, u32[]{:S(2)}) copy-start(bf16[128,2048]{1,0:T(8,128)(2,1)} %refs_0_.1) | copy-start | bytes 1572868
  8.4 10.4 %collective-permute-start.2 = (bf16[80,1024]{1,0:T(8,128)(2,1)}, bf16[80,1024]{1,0:T(8,128)(2,1)S(1)}, u32[]{:S(2)}, u32[]{:S(2)}) collective-permute-start(bf16[80,1024]{1,0:T(8,128)(2,1)} %states.1.own_ref), channel_id=1, source_target_pairs={{0,24},{8,0},{16,8},{24,16},{1,25},{9,1},{17,9},{25,17},{2,26},{10... | collective-permute-start | bytes 491528 | tf_op jit(solution)/shard_map/ppermute | solution.py:372
  11.6 8.8 %collective-permute-start.1 = (bf16[80,1024]{1,0:T(8,128)(2,1)}, bf16[80,1024]{1,0:T(8,128)(2,1)S(1)}, u32[]{:S(2)}, u32[]{:S(2)}) collective-permute-start(bf16[80,1024]{1,0:T(8,128)(2,1)} %states.1.own_ref), channel_id=1, source_target_pairs={{0,16},{8,24},{16,0},{24,8},{1,17},{9,25},{17,1},{25,9},{2,18},{10... | collective-permute-start | bytes 491528 | tf_op jit(solution)/shard_map/ppermute | solution.py:372
  12.2 10.3 %collective-permute-start = (bf16[80,1024]{1,0:T(8,128)(2,1)}, bf16[80,1024]{1,0:T(8,128)(2,1)S(1)}, u32[]{:S(2)}, u32[]{:S(2)}) collective-permute-start(bf16[80,1024]{1,0:T(8,128)(2,1)} %states.1.own_ref), channel_id=1, source_target_pairs={{0,8},{8,16},{16,24},{24,0},{1,9},{9,17},{17,25},{25,1},{2,10},{10... | collective-permute-start | bytes 491528 | tf_op jit(solution)/shard_map/ppermute | solution.py:372
  13.2 24.4 %collective-permute-start.5 = (bf16[128,2048]{1,0:T(8,128)(2,1)S(1)}, bf16[128,2048]{1,0:T(8,128)(2,1)S(1)}, u32[]{:S(2)}, u32[]{:S(2)}) collective-permute-start(bf16[128,2048]{1,0:T(8,128)(2,1)S(1)} %copy-done.2), channel_id=1, source_target_pairs={{0,6},{2,0},{4,2},{6,4},{1,7},{3,1},{5,3},{7,5},{8,14},{10,8},{12,... | collective-permute-start | bytes 1572872 | tf_op jit(solution)/shard_map/ppermute | solution.py:357
  15.9 21.6 %collective-permute-start.4 = (bf16[128,2048]{1,0:T(8,128)(2,1)S(1)}, bf16[128,2048]{1,0:T(8,128)(2,1)S(1)}, u32[]{:S(2)}, u32[]{:S(2)}) collective-permute-start(bf16[128,2048]{1,0:T(8,128)(2,1)S(1)} %copy-done.2), channel_id=1, source_target_pairs={{0,4},{2,6},{4,0},{6,2},{1,5},{3,7},{5,1},{7,3},{8,12},{10,14},{12... | collective-permute-start | bytes 1572872 | tf_op jit(solution)/shard_map/ppermute | solution.py:357
  18.8 3.6 %copy-start.13 = (bf16[80,1024]{1,0:T(8,128)(2,1)}, bf16[80,1024]{1,0:T(8,128)(2,1)S(1)}, u32[]{:S(2)}) copy-start(bf16[80,1024]{1,0:T(8,128)(2,1)S(1)} %collective-permute-done.2.three_ref) | copy-start | bytes 491524
  18.8 22.4 %collective-permute-start.3 = (bf16[128,2048]{1,0:T(8,128)(2,1)S(1)}, bf16[128,2048]{1,0:T(8,128)(2,1)S(1)}, u32[]{:S(2)}, u32[]{:S(2)}) collective-permute-start(bf16[128,2048]{1,0:T(8,128)(2,1)S(1)} %copy-done.2), channel_id=1, source_target_pairs={{0,2},{2,4},{4,6},{6,0},{1,3},{3,5},{5,7},{7,1},{8,10},{10,12},{12... | collective-permute-start | bytes 1572872 | tf_op jit(solution)/shard_map/ppermute | solution.py:357
  20.4 2.1 copy-start.14
  20.4 45.8 %collective-permute-start.9 = (bf16[128,2048]{1,0:T(8,128)(2,1)S(1)}, bf16[128,2048]{1,0:T(8,128)(2,1)S(1)}, u32[]{:S(2)}, u32[]{:S(2)}) collective-permute-start(bf16[128,2048]{1,0:T(8,128)(2,1)S(1)} %copy-done.2), channel_id=1, source_target_pairs={{0,1},{1,0},{2,3},{3,2},{4,5},{5,4},{6,7},{7,6},{8,9},{9,8},{10,11... | collective-permute-start | bytes 1572872 | tf_op jit(solution)/shard_map/ppermute | solution.py:405
  25.2 35.0 %copy-start.11 = (s32[1,384,2]{1,2,0:T(2,128)S(1)}, s32[1,384,2]{1,2,0:T(2,128)}, u32[]{:S(2)}) copy-start(s32[1,384,2]{1,2,0:T(2,128)} %param.26) | copy-start | bytes 9220
  41.2 25.0 %collective-permute-start.10 = (bf16[128,2048]{1,0:T(8,128)(2,1)S(1)}, bf16[128,2048]{1,0:T(8,128)(2,1)S(1)}, u32[]{:S(2)}, u32[]{:S(2)}) collective-permute-start(bf16[128,2048]{1,0:T(8,128)(2,1)S(1)} %collective-permute-done.3.refs_1_), channel_id=1, source_target_pairs={{0,1},{1,0},{2,3},{3,2},{4,5},{5,4},{6,7},{7,6},{8,9},{9,8},{10,11... | collective-permute-start | bytes 1572872 | tf_op jit(solution)/shard_map/ppermute | solution.py:405
  41.2 25.0 %collective-permute-start.11 = (bf16[128,2048]{1,0:T(8,128)(2,1)S(1)}, bf16[128,2048]{1,0:T(8,128)(2,1)}, u32[]{:S(2)}, u32[]{:S(2)}) collective-permute-start(bf16[128,2048]{1,0:T(8,128)(2,1)S(1)} %collective-permute-done.4.refs_2_), channel_id=1, source_target_pairs={{0,1},{1,0},{2,3},{3,2},{4,5},{5,4},{6,7},{7,6},{8,9},{9,8},{10,11... | collective-permute-start | bytes 1572872 | tf_op jit(solution)/shard_map/ppermute | solution.py:405
  41.7 24.5 %collective-permute-start.12 = (bf16[128,2048]{1,0:T(8,128)(2,1)S(1)}, bf16[128,2048]{1,0:T(8,128)(2,1)}, u32[]{:S(2)}, u32[]{:S(2)}) collective-permute-start(bf16[128,2048]{1,0:T(8,128)(2,1)S(1)} %collective-permute-done.5.refs_3_), channel_id=1, source_target_pairs={{0,1},{1,0},{2,3},{3,2},{4,5},{5,4},{6,7},{7,6},{8,9},{9,8},{10,11... | collective-permute-start | bytes 1572872 | tf_op jit(solution)/shard_map/ppermute | solution.py:405
  41.7 8.5 %collective-permute-start.8 = (bf16[80,1024]{1,0:T(8,128)(2,1)}, bf16[80,1024]{1,0:T(8,128)(2,1)S(1)}, u32[]{:S(2)}, u32[]{:S(2)}) collective-permute-start(bf16[80,1024]{1,0:T(8,128)(2,1)} %get-tuple-element.23), channel_id=1, source_target_pairs={{0,96},{32,0},{64,32},{96,64},{1,97},{33,1},{65,33},{97,65},{2,98}... | collective-permute-start | bytes 491528 | tf_op jit(solution)/shard_map/ppermute | solution.py:390
  50.9 7.5 %collective-permute-start.7 = (bf16[80,1024]{1,0:T(8,128)(2,1)}, bf16[80,1024]{1,0:T(8,128)(2,1)S(1)}, u32[]{:S(2)}, u32[]{:S(2)}) collective-permute-start(bf16[80,1024]{1,0:T(8,128)(2,1)} %get-tuple-element.23), channel_id=1, source_target_pairs={{0,64},{32,96},{64,0},{96,32},{1,65},{33,97},{65,1},{97,33},{2,66}... | collective-permute-start | bytes 491528 | tf_op jit(solution)/shard_map/ppermute | solution.py:390
  59.0 7.2 %collective-permute-start.6 = (bf16[80,1024]{1,0:T(8,128)(2,1)}, bf16[80,1024]{1,0:T(8,128)(2,1)}, u32[]{:S(2)}, u32[]{:S(2)}) collective-permute-start(bf16[80,1024]{1,0:T(8,128)(2,1)} %get-tuple-element.23), channel_id=1, source_target_pairs={{0,32},{32,64},{64,96},{96,0},{1,33},{33,65},{65,97},{97,1},{2,34}... | collective-permute-start | bytes 491528 | tf_op jit(solution)/shard_map/ppermute | solution.py:390
  60.2 22.8 %copy-start.1 = (s32[8,384]{1,0:T(8,128)}, s32[8,384]{1,0:T(8,128)S(1)}, u32[]{:S(2)}) copy-start(s32[8,384]{1,0:T(8,128)S(1)} %pad.8.refs_9_.routes_ref) | copy-start | bytes 36868
  66.2 0.9 copy-start.4
  68.8 0.9 copy-start.8
  159.9 12.5 %copy-start.12 = (f32[1,384,2]{1,2,0:T(2,128)S(1)}, f32[1,384,2]{1,2,0:T(2,128)}, u32[]{:S(2)}) copy-start(f32[1,384,2]{1,2,0:T(2,128)} %param.27) | copy-start | bytes 9220
  168.7 33.4 %all-to-all-start.2 = ((bf16[16,16,2048]{2,1,0:T(8,128)(2,1)}), bf16[16,16,2048]{2,1,0:T(8,128)(2,1)S(1)}, u32[]{:S(2)}, u32[]{:S(2)}) async-start(bf16[16,16,2048]{2,1,0:T(8,128)(2,1)} %serve.2), calls=%async_computation.2 | async-start | bytes 2097152 | tf_op jit(solution)/shard_map/all_to_all | solution.py:458
  202.1 66.2 %copy-start.10 = (bf16[16,16,2048]{2,1,0:T(8,128)(2,1)}, bf16[16,16,2048]{2,1,0:T(8,128)(2,1)S(1)}, u32[]{:S(2)}) copy-start(bf16[16,16,2048]{2,1,0:T(8,128)(2,1)S(1)} %all-to-all-done.2) | copy-start | bytes 3145732
  (6 other events, 4.4 us)

commit v2 on v1

--- a/solution.py
+++ b/solution.py
@@ -192,7 +192,7 @@
 ):
     wmine = refs[0:4]
     wother = refs[4:8]
-    scale_ref, routes_ref, upd_ref, send_ref, w_s, state_s, norm_s, pos_s = refs[8:]
+    scale_ref, routes_ref, upd_ref, send_ref, w_s, state_s, norm_s, pos_s, sems = refs[8:]
 
     step = pl.program_id(0)
     width = gate_ref.shape[1]
@@ -200,8 +200,19 @@
     tok_rows = routes_ref.shape[1]
     rows = gate_ref.shape[0]
 
+    piece = wmine[0].shape[0]
+
+    def weight_copies():
+        for n in range(4):
+            src = (pos_ref[1] + 4 - n) % 4
+            for i, (ref, core) in enumerate(((wmine[n], pos_ref[2]), (wother[n], 1 - pos_ref[2]))):
+                where = pl.ds(pl.multiple_of((2 * src + core) * piece, piece), piece)
+                yield pltpu.make_async_copy(ref, w_s.at[where], sems.at[2 * n + i])
+
     @pl.when(step == 0)
     def _():
+        for c in weight_copies():
+            c.start()
         here = pos_ref[0]
         state = jnp.zeros((CH, width), F32)
         for n, ref in ((3, three_ref), (2, two_ref), (1, one_ref)):
@@ -213,13 +224,6 @@
         for g in range(groups):
             one = state[:, g * GL : (g + 1) * GL]
             state_s[g] = jnp.where(mask, jnp.concatenate([one] * 4, axis=0), jnp.zeros((GL, GL), BF))
-        x_here = pos_ref[1]
-        core = pos_ref[2]
-        piece = wmine[0].shape[0]
-        for n in range(4):
-            src = (x_here + 4 - n) % 4
-            w_s[pl.ds((2 * src + core) * piece, piece), :] = wmine[n][...]
-            w_s[pl.ds((2 * src + 1 - core) * piece, piece), :] = wother[n][...]
         experts = pos_s.shape[0]
         e = lax.broadcasted_iota(jnp.int32, (experts, tok_rows), 0)
         member = (e == routes_ref[0:1, :]) | (e == routes_ref[1:2, :])
@@ -243,6 +247,12 @@
             gate = silu(gate_ref[:, lanes].astype(F32))
             mixed.append((o * lax.rsqrt(mean + 1e-06) * gate).astype(BF))
         mixed = jnp.concatenate(mixed, axis=1)
+
+        @pl.when(step == 0)
+        def _():
+            for c in weight_copies():
+                c.wait()
+
         upd = (res_ref[...].astype(F32) + dot(mixed, w_s[...])).astype(BF)
         upd_ref[...] = upd
         wide = upd.astype(F32)
@@ -261,21 +271,125 @@
         send_ref[...] = dot(jnp.concatenate(picks, axis=0), norm_s[...]).astype(BF)
 
 
-def serve_kernel(hid_steps, x_ref, wg_ref, wu_ref, wd_ref, out_ref, hid_s):
-    step = pl.program_id(1)
-    blk = wg_ref.shape[2]
-
-    for n in range(hid_steps):
-
-        @pl.when(step == n)
-        def _(n=n):
-            x = x_ref[...].reshape(hid_s.shape[0], x_ref.shape[2])
-            hidden = silu(dot(x, wg_ref[0])) * dot(x, wu_ref[0])
-            hid_s[:, n * blk : (n + 1) * blk] = hidden.astype(BF)
-
-    @pl.when(step >= hid_steps)
-    def _():
-        out_ref[...] = dot(hid_s[...], wd_ref[0]).astype(BF).reshape(out_ref.shape)
+def serve_kernel(
+    first, parts, x_ref, wg_ref, wu_ref, wd_ref, out_ref, x_s, wg_s, wu_s, wd_s, hid_s, out_s, sems, out_sems
+):
+    srcs, size, model = x_s.shape
+    hid = hid_s.shape[1]
+    steps = 4
+    hb = hid // steps
+    ob = model // steps
+    per = srcs // parts
+    rows = per * size
+
+    def x_copy(m):
+        lo = m * per
+        return pltpu.make_async_copy(
+            x_ref.at[pl.ds(lo, per), pl.ds(first, size), :], x_s.at[pl.ds(lo, per)], sems.at[m]
+        )
+
+    def w_copy(which, n):
+        src, dst, cols = ((wg_ref, wg_s, hb), (wu_ref, wu_s, hb), (wd_ref, wd_s, ob))[which]
+        lanes = pl.ds(n * cols, cols)
+        return pltpu.make_async_copy(
+            src.at[0, :, lanes], dst.at[:, lanes], sems.at[parts + which * steps + n]
+        )
+
+    def out_copy(m, n):
+        lanes = pl.ds(n * ob, ob)
+        return pltpu.make_async_copy(
+            out_s.at[pl.ds(m * per, per), :, lanes],
+            out_ref.at[pl.ds(m * per, per), :, lanes],
+            out_sems.at[m * steps + n],
+        )
+
+    x_copy(0).start()
+    w_copy(0, 0).start()
+    w_copy(1, 0).start()
+    for m in range(1, parts):
+        x_copy(m).start()
+    x_copy(0).wait()
+    w_copy(0, 0).wait()
+    w_copy(1, 0).wait()
+    for n in range(1, steps):
+        w_copy(0, n).start()
+        w_copy(1, n).start()
+    for n in range(steps):
+        w_copy(2, n).start()
+    for n in range(steps):
+        lanes = slice(n * hb, (n + 1) * hb)
+        if n > 0:
+            w_copy(0, n).wait()
+            w_copy(1, n).wait()
+        for m in range(parts):
+            if n == 0 and m > 0:
+                x_copy(m).wait()
+            x = x_s[m * per : (m + 1) * per].reshape(rows, model)
+            hidden = silu(dot(x, wg_s[:, lanes])) * dot(x, wu_s[:, lanes])
+            hid_s[m * rows : (m + 1) * rows, lanes] = hidden.astype(BF)
+    for n in range(steps):
+        lanes = slice(n * ob, (n + 1) * ob)
+        w_copy(2, n).wait()
+        for m in range(parts):
+            got = dot(hid_s[m * rows : (m + 1) * rows, :], wd_s[:, lanes]).astype(BF)
+            out_s[m * per : (m + 1) * per, :, lanes] = got.reshape(per, size, ob)
+            out_copy(m, n).start()
+    for n in range(steps):
+        for m in range(parts):
+            out_copy(m, n).wait()
+
+
+def serve_rest_kernel(
+    first, parts, x_ref, wg_ref, wu_ref, wd_ref, out_ref, x_s, wd_s, hid_s, out_s, sems, wd_sems, out_sems
+):
+    srcs, size, model = x_s.shape
+    hid = hid_s.shape[1]
+    steps = 4
+    hb = hid // steps
+    ob = model // steps
+    per = srcs // parts
+    rows = per * size
+
+    def x_copy(m):
+        lo = m * per
+        return pltpu.make_async_copy(
+            x_ref.at[pl.ds(lo, per), pl.ds(first, size), :], x_s.at[pl.ds(lo, per)], sems.at[m]
+        )
+
+    def wd_copy(n):
+        lanes = pl.ds(n * ob, ob)
+        return pltpu.make_async_copy(wd_ref.at[0, :, lanes], wd_s.at[:, lanes], wd_sems.at[n])
+
+    def out_copy(m, n):
+        lanes = pl.ds(n * ob, ob)
+        return pltpu.make_async_copy(
+            out_s.at[pl.ds(m * per, per), :, lanes],
+            out_ref.at[pl.ds(m * per, per), :, lanes],
+            out_sems.at[m * steps + n],
+        )
+
+    for m in range(parts):
+        x_copy(m).start()
+    for n in range(steps):
+        wd_copy(n).start()
+    for n in range(steps):
+        lanes = slice(n * hb, (n + 1) * hb)
+        for m in range(parts):
+            if n == 0:
+                x_copy(m).wait()
+            x = x_s[m * per : (m + 1) * per].reshape(rows, model)
+            hidden = silu(dot(x, wg_ref[0, :, lanes])) * dot(x, wu_ref[0, :, lanes])
+            hid_s[m * rows : (m + 1) * rows, lanes] = hidden.astype(BF)
+    for n in range(steps):
+        lanes = slice(n * ob, (n + 1) * ob)
+        wd_copy(n).wait()
+        for m in range(parts):
+            got = dot(hid_s[m * rows : (m + 1) * rows, :], wd_s[:, lanes]).astype(BF)
+            out_s[m * per : (m + 1) * per, :, lanes] = got.reshape(per, size, ob)
+            out_copy(m, n).start()
+    for n in range(steps):
+        for m in range(parts):
+            out_copy(m, n).wait()
 
 
 def weights_kernel(main, routes_ref, wt_ref, main_ref, rest_ref):
@@ -302,9 +416,21 @@
         ref[...] = weight.astype(BF)
 
 
-def combine_kernel(main_ref, rest_ref, got_ref, got_rest_ref, upd_ref, out_ref):
-    total = dot(main_ref[...], got_ref[...]) + dot(rest_ref[...], got_rest_ref[...])
-    out_ref[...] = (upd_ref[...].astype(F32) + total).astype(out_ref.dtype)
+def combine_kernel(main_ref, rest_ref, got_ref, got_rest_ref, upd_ref, out_ref, out_s, sems):
+    steps = sems.shape[0]
+    blk = out_s.shape[1] // steps
+
+    def out_copy(n):
+        lanes = pl.ds(n * blk, blk)
+        return pltpu.make_async_copy(out_s.at[:, lanes], out_ref.at[:, lanes], sems.at[n])
+
+    for n in range(steps):
+        lanes = slice(n * blk, (n + 1) * blk)
+        total = dot(main_ref[...], got_ref[:, lanes]) + dot(rest_ref[...], got_rest_ref[:, lanes])
+        out_s[:, lanes] = (upd_ref[:, lanes].astype(F32) + total).astype(out_s.dtype)
+        out_copy(n).start()
+    for n in range(steps):
+        out_copy(n).wait()
 
 
 def cost(us):
@@ -366,6 +492,7 @@
         out_specs=pl.BlockSpec((PACK, GL), lambda g: (0, g)),
         out_shape=jax.ShapeDtypeStruct((PACK, width), BF),
         cost_estimate=cost(7),
+        compiler_params=pltpu.CompilerParams(vmem_limit_bytes=66 * 1000 * 1000),
         name="states",
     )(f, v, floor, spikes)
 
@@ -374,6 +501,18 @@
 
     vm = pl.BlockSpec(memory_space=pltpu.VMEM)
     sm = pl.BlockSpec(memory_space=pltpu.SMEM)
+
+    inside, qrun = pl.pallas_call(
+        inside_kernel,
+        grid=(groups,),
+        in_specs=[tall, tall, tall, flat, whole],
+        out_specs=[tall, tall],
+        out_shape=[jax.ShapeDtypeStruct((tok, width), F32), jax.ShapeDtypeStruct((tok, width), BF)],
+        cost_estimate=cost(8),
+        compiler_params=pltpu.CompilerParams(vmem_limit_bytes=66 * 1000 * 1000),
+        name="inside",
+    )(q, f, v, floor, spikes)
+
     row, before, btot = pl.pallas_call(
         row_kernel,
         in_specs=[sm, vm, vm, vm, vm],
@@ -384,28 +523,33 @@
             jax.ShapeDtypeStruct((8, width), F32),
         ],
         cost_estimate=cost(2),
+        compiler_params=pltpu.CompilerParams(vmem_limit_bytes=66 * 1000 * 1000),
         name="row",
     )(y.astype(jnp.int32).reshape(1), pack, *along_y)
 
     along_z = [lax.ppermute(row, "sp_0", ring(n)) for n in (1, 2, 3)]
 
-    q, row = lax.optimization_barrier((q, row))
-    inside, qrun = pl.pallas_call(
-        inside_kernel,
-        grid=(groups,),
-        in_specs=[tall, tall, tall, flat, whole],
-        out_specs=[tall, tall],
-        out_shape=[jax.ShapeDtypeStruct((tok, width), F32), jax.ShapeDtypeStruct((tok, width), BF)],
-        cost_estimate=cost(8),
-        name="inside",
-    )(q, f, v, floor, spikes)
-
-    wmine, qrun = lax.optimization_barrier((wmine, qrun))
+    wmine, row = lax.optimization_barrier((wmine, row))
     wmine = [mine] + wmine
     wother = [lax.ppermute(p, "c", ring(1, 2)) for p in wmine]
 
-
     route_rows = jnp.pad(routes[0].T, ((0, 6), (0, 0)), constant_values=-1)
+    wt_rows = jnp.pad(routing_weight[0].T, ((0, 6), (0, 0)))
+    route_rows, wt_rows, row = lax.optimization_barrier((route_rows, wt_rows, row))
+    weights_main, weights_rest = pl.pallas_call(
+        functools.partial(weights_kernel, main),
+        in_specs=[vm, vm],
+        out_specs=[vm, vm],
+        out_shape=[
+            jax.ShapeDtypeStruct((tok, experts * main), BF),
+            jax.ShapeDtypeStruct((tok, experts * rest), BF),
+        ],
+        cost_estimate=cost(2),
+        compiler_params=pltpu.CompilerParams(vmem_limit_bytes=66 * 1000 * 1000),
+        name="weights",
+    )(route_rows, wt_rows)
+
+
     place = jnp.stack([z, x, core]).astype(jnp.int32)
     tok_steps = 3
     rows = tok // tok_steps
@@ -431,7 +575,7 @@
             full(row),
             full(row),
             full(row),
-            *[full(mine)] * 8,
+            *[pl.BlockSpec(memory_space=pl.ANY)] * 8,
             full(scale),
             full(route_rows),
         ],
@@ -448,8 +592,9 @@
             pltpu.VMEM((groups, GL, GL), BF),
             pltpu.VMEM((tok, model), BF),
             pltpu.VMEM((experts, tok), jnp.int32),
+            pltpu.SemaphoreType.DMA((8,)),
         ],
-        compiler_params=pltpu.CompilerParams(vmem_limit_bytes=50 * 1024 * 1024),
+        compiler_params=pltpu.CompilerParams(vmem_limit_bytes=66 * 1000 * 1000),
         cost_estimate=cost(12),
         name="mix",
     )(place, inside, qrun, gate, res, before, btot, *along_z, *wmine, *wother, scale, route_rows)
@@ -458,68 +603,50 @@
         return lax.all_to_all(a, SP, split_axis=0, concat_axis=0, tiled=True)
 
     hid = expert_gate_weight.shape[2]
-    hid_steps = 2
-    out_steps = 2
-
-    def serve(arrived, first, size, blocks):
-        srcs = experts // blocks
-        where = first // size
-        up = pl.BlockSpec(
-            (1, model, hid // hid_steps), lambda m, j: (0, 0, jnp.minimum(j, hid_steps - 1))
-        )
-        after = lambda j: jnp.maximum(j - hid_steps, 0)
+    anywhere = pl.BlockSpec(memory_space=pl.ANY)
+
+    dma = lambda n: pltpu.SemaphoreType.DMA((n,))
+
+    def serve(kernel, arrived, first, size, parts, scratch, specs, limit, us):
         return pl.pallas_call(
-            functools.partial(serve_kernel, hid_steps),
-            grid=(blocks, hid_steps + out_steps),
-            in_specs=[
-                pl.BlockSpec((srcs, size, model), lambda m, j: (m, where, 0)),
-                up,
-                up,
-                pl.BlockSpec((1, hid, model // out_steps), lambda m, j: (0, 0, after(j))),
+            functools.partial(kernel, first, parts),
+            in_specs=[anywhere, *specs],
+            out_specs=anywhere,
+            out_shape=jax.ShapeDtypeStruct((experts, size, model), BF),
+            scratch_shapes=[
+                pltpu.VMEM((experts, size, model), BF),
+                *[pltpu.VMEM(shape, BF) for shape in scratch],
+                pltpu.VMEM((experts * size, hid), BF),
+                pltpu.VMEM((experts, size, model), BF),
+                *([dma(parts), dma(4)] if kernel is serve_rest_kernel else [dma(parts + 12)]),
+                dma(parts * 4),
             ],
-            out_specs=pl.BlockSpec((srcs, size, model // out_steps), lambda m, j: (m, 0, after(j))),
-            out_shape=jax.ShapeDtypeStruct((experts, size, model), BF),
-            scratch_shapes=[pltpu.VMEM((srcs * size, hid), BF)],
-            compiler_params=pltpu.CompilerParams(vmem_limit_bytes=50 * 1024 * 1024),
-            cost_estimate=cost(18 if blocks > 1 else 5),
+            compiler_params=pltpu.CompilerParams(vmem_limit_bytes=limit * 1024 * 1024),
+            cost_estimate=cost(us),
             name="serve",
         )(arrived, expert_gate_weight, expert_up_weight, expert_down_weight)
 
+    def serve_main(arrived):
+        scratch = [(model, hid), (model, hid), (hid, model)]
+        return serve(serve_kernel, arrived, 0, main, 2, scratch, [anywhere] * 3, 50, 20)
+
+    def serve_rest(arrived):
+        specs = [vm, vm, anywhere]
+        return serve(serve_rest_kernel, arrived, main, rest, 1, [(hid, model)], specs, 36, 5)
+
     arrived = exchange(send.reshape(experts, cap, model))
-    served_rest = serve(arrived, main, rest, 1)
+    served_rest = serve_rest(arrived)
     got_rest = exchange(served_rest)
 
-    picks, _ = lax.optimization_barrier((route_rows, served_rest))
-    weights_main, weights_rest = pl.pallas_call(
-        functools.partial(weights_kernel, main),
-        in_specs=[vm, vm],
-        out_specs=[vm, vm],
-        out_shape=[
-            jax.ShapeDtypeStruct((tok, experts * main), BF),
-            jax.ShapeDtypeStruct((tok, experts * rest), BF),
-        ],
-        cost_estimate=cost(2),
-        name="weights",
-    )(picks, jnp.pad(routing_weight[0].T, ((0, 6), (0, 0))))
-    arrived, weights_main, weights_rest = lax.optimization_barrier(
-        (arrived, weights_main, weights_rest)
-    )
-    got = exchange(serve(arrived, 0, main, 2))
-
-    blk = 512
-    col = lambda r: pl.BlockSpec((r, blk), lambda i: (0, i))
+    got = exchange(serve_main(arrived))
+
     layer_out = pl.pallas_call(
         combine_kernel,
-        grid=(model // blk,),
-        in_specs=[
-            full(weights_main),
-            full(weights_rest),
-            col(experts * main),
-            col(experts * rest),
-            col(tok),
-        ],
-        out_specs=col(tok),
+        in_specs=[vm] * 5,
+        out_specs=anywhere,
         out_shape=jax.ShapeDtypeStruct((tok, model), BF),
+        scratch_shapes=[pltpu.VMEM((tok, model), BF), pltpu.SemaphoreType.DMA((4,))],
+        compiler_params=pltpu.CompilerParams(vmem_limit_bytes=40 * 1024 * 1024),
         cost_estimate=cost(4),
         name="combine",
     )(

time: 276 us -> 274 us (level)
  blocking collectives: 143 us -> 80.2 us
  waiting for transfers between devices: 27.5 us -> 89.1 us
  Pallas kernels: 74.6 us -> 68.2 us
  starting transfers between devices: 21.4 us -> 26.6 us
    all_to_all x1 -> x2, waiting for transfers between devices: 0.01 us -> 72.6 us  [exchange(): return lax.all_to_all(a, SP, split_axis=0, concat_axis=0, tiled=True)]
    all_to_all x2 -> x1, blocking collectives: 143 us -> 80.2 us  [exchange(): return lax.all_to_all(a, SP, split_axis=0, concat_axis=0, tiled=True)]
    ppermute x3, waiting for transfers between devices: 15.6 us -> 0.01 us  [per_device(): along_z = [lax.ppermute(row, 'sp_0', ring(n)) for n in (1, 2, 3)]]
    pallas_call x3, Pallas kernels: 41.6 us -> 33.6 us  [the longest x2 27.7 us: serve(): pl.pallas_call(functools.partial(kernel, first, parts), in_specs=[anywher...]
    all_to_all x1 -> x2, starting transfers between devices: 3.66 us -> 10.9 us  [exchange(): return lax.all_to_all(a, SP, split_axis=0, concat_axis=0, tiled=True)]
    ppermute x3, waiting for transfers between devices: 4.22 us -> 8.55 us  [per_device(): along_y = [lax.ppermute(pack, 'sp_1', ring(n)) for n in (1, 2, 3)]]
    unnamed x32 -> x28, local copies, waits for them, and re-layouts: 7.25 us -> 6.76 us
  transfers between devices with their start and end apart: 14 -> 15, of which waited for: 8 -> 5; matrix products, arithmetic and copies ran while one was open for 0% -> 1% of each run, Pallas kernels for 14% -> 13%
where the time goes in v2:
time: 274 us
  waiting for transfers between devices  89.1 us (33%)
  blocking collectives  80.2 us (29%)
  Pallas kernels  68.2 us (25%)
  starting transfers between devices  26.6 us (10%)
  local copies, waits for them, and re-layouts  8.57 us (3%)
    all_to_all x1, blocking collectives, exchange(): return lax.all_to_all(a, SP, split_axis=0, concat_axis=0, tiled=True)  80.2 us
    all_to_all x2, waiting for transfers between devices, exchange(): return lax.all_to_all(a, SP, split_axis=0, concat_axis=0, tiled=True)  72.6 us
    pallas_call x2, Pallas kernels, serve(): pl.pallas_call(functools.partial(kernel, first, parts), in_specs=[anywher...  27.7 us
    pallas_call x1, Pallas kernels, per_device(): pl.pallas_call(functools.partial(mix_kernel, tok_steps, cap), grid=(tok_s...  14.1 us
    all_to_all x2, starting transfers between devices, exchange(): return lax.all_to_all(a, SP, split_axis=0, concat_axis=0, tiled=True)  10.9 us
    ppermute x3, waiting for transfers between devices, per_device(): along_y = [lax.ppermute(pack, 'sp_1', ring(n)) for n in (1, 2, 3)]  8.55 us
    pallas_call x1, Pallas kernels, per_device(): pl.pallas_call(inside_kernel, grid=(groups,), in_specs=[tall, tall, tall,...  8.26 us
    ppermute x3, waiting for transfers between devices, per_device(): wmine = [lax.ppermute(mine, 'x', ring(n)) for n in (1, 2, 3)]  7.93 us
  transfers between devices with their start and end apart: 15, of which 5 were waited for; matrix products, arithmetic and copies ran while one was open for 1% of the time, Pallas kernels for 13%

profile of v2, /device:TPU:0, one launch (start us, length us, event | category | flops | bytes accessed | tf_op | source)
XLA Modules:
  0.0 273.6 jit_solution(6432753054586639113)
XLA Ops:
  0.0 1.0 copy-done
  1.6 6.8 %states.1.own_ref = bf16[80,1024]{1,0:T(8,128)(2,1)} custom-call(bf16[384,1024]{1,0:T(8,128)(2,1)} %bitcast.31, bf16[384,1024]{1,0:T(8,128)(2,1)} %bitcast.33, f32[1,1024]{1,0:T(1,128)} %bitcast.37, f32[16,384]{1,0:T(8,128)} %dynamic-slice_bitcast_fusion.spike_ref), custom_call_target="tpu_custom_call" | custom-call | flops 3500000000 | bytes 7000000 | tf_op jit(solution)/shard_map/states/pallas_call | solution.py:488
  8.4 3.1 %collective-permute-start.2 = (bf16[80,1024]{1,0:T(8,128)(2,1)}, bf16[80,1024]{1,0:T(8,128)(2,1)}, u32[]{:S(2)}, u32[]{:S(2)}) collective-permute-start(bf16[80,1024]{1,0:T(8,128)(2,1)} %states.1.own_ref), channel_id=1, source_target_pairs={{0,24},{8,0},{16,8},{24,16},{1,25},{9,1},{17,9},{25,17},{2,26},{10... | collective-permute-start | bytes 491528 | tf_op jit(solution)/shard_map/ppermute | solution.py:499
  11.6 2.8 %collective-permute-start.8 = (bf16[128,2048]{1,0:T(8,128)(2,1)S(1)}, bf16[128,2048]{1,0:T(8,128)(2,1)}, u32[]{:S(2)}, u32[]{:S(2)}) collective-permute-start(bf16[128,2048]{1,0:T(8,128)(2,1)S(1)} %copy-done.11), channel_id=1, source_target_pairs={{0,6},{2,0},{4,2},{6,4},{1,7},{3,1},{5,3},{7,5},{8,14},{10,8},{12,... | collective-permute-start | bytes 1572872 | tf_op jit(solution)/shard_map/ppermute | solution.py:483
  17.6 6.8 %collective-permute-done.1.two_ref = bf16[80,1024]{1,0:T(8,128)(2,1)} collective-permute-done((bf16[80,1024]{1,0:T(8,128)(2,1)}, bf16[80,1024]{1,0:T(8,128)(2,1)}, u32[]{:S(2)}, u32[]{:S(2)}) %collective-permute-start.1) | collective-permute-done | bytes 163872 | tf_op jit(solution)/shard_map/ppermute | solution.py:499
  24.4 1.7 collective-permute-done.one_ref
  26.2 2.1 row.1
  28.3 4.0 %collective-permute-start.5 = (bf16[80,1024]{1,0:T(8,128)(2,1)}, bf16[80,1024]{1,0:T(8,128)(2,1)S(1)}, u32[]{:S(2)}, u32[]{:S(2)}) collective-permute-start(bf16[80,1024]{1,0:T(8,128)(2,1)} %get-tuple-element.27), channel_id=1, source_target_pairs={{0,96},{32,0},{64,32},{96,64},{1,97},{33,1},{65,33},{97,65},{2,98}... | collective-permute-start | bytes 491528 | tf_op jit(solution)/shard_map/ppermute | solution.py:530
  32.3 4.2 %collective-permute-done.8.refs_3_ = bf16[128,2048]{1,0:T(8,128)(2,1)} collective-permute-done((bf16[128,2048]{1,0:T(8,128)(2,1)S(1)}, bf16[128,2048]{1,0:T(8,128)(2,1)}, u32[]{:S(2)}, u32[]{:S(2)}) %collective-permute-start.8) | collective-permute-done | bytes 524320 | tf_op jit(solution)/shard_map/ppermute | solution.py:483
  36.5 3.8 %collective-permute-done.6.refs_1_ = bf16[128,2048]{1,0:T(8,128)(2,1)} collective-permute-done((bf16[128,2048]{1,0:T(8,128)(2,1)S(1)}, bf16[128,2048]{1,0:T(8,128)(2,1)}, u32[]{:S(2)}, u32[]{:S(2)}) %collective-permute-start.6) | collective-permute-done | bytes 524320 | tf_op jit(solution)/shard_map/ppermute | solution.py:483
  40.9 1.9 collective-permute-start.3
  42.8 8.3 %inside.1 = (f32[384,1024]{1,0:T(8,128)}, bf16[384,1024]{1,0:T(8,128)(2,1)}) custom-call(bf16[384,1024]{1,0:T(8,128)(2,1)} %bitcast.30, bf16[384,1024]{1,0:T(8,128)(2,1)} %bitcast.32, bf16[384,1024]{1,0:T(8,128)(2,1)} %bitcast.34, f32[1,1024]{1,0:T(1,128)} %bitcast.38, f32[16,384]{1,0:T(8,128)} %dynamic-slice_bitcast_fusion.spike_ref), custom_call_target="tpu_custom_call" | custom-call | flops 4000000000 | bytes 8000000 | tf_op jit(solution)/shard_map/inside/pallas_call | solution.py:505
  52.9 14.1 %mix.1 = (bf16[384,2048]{1,0:T(8,128)(2,1)}, bf16[1536,2048]{1,0:T(8,128)(2,1)}) custom-call(s32[3]{0:T(128)} %pad_add_fusion.pos_ref, f32[384,1024]{1,0:T(8,128)} %get-tuple-element.23.out_ref, bf16[384,1024]{1,0:T(8,128)(2,1)} %get-tuple-element.24.qrun_ref, bf16[384,1024]{1,0:T(8,128)(2,1)} %bitcast.35, bf16[384,2048]{1,0:T(8,128)(2,1)} %bitcast.29, ...), custom_call_target="tpu_custom_call" | custom-call | flops 6000000000 | bytes 12000000 | tf_op jit(solution)/shard_map/mix/pallas_call | solution.py:564
  67.1 80.2 %all_to_all.15.x_ref = bf16[16,96,2048]{2,1,0:T(8,128)(2,1)} all-to-all(bf16[16,96,2048]{2,1,0:T(8,128)(2,1)} %bitcast.26), channel_id=1, replica_groups=mesh['sp_0'=4,'sp_1'=4,'x'=4,'c'=2] {'sp_0','sp_1'}, dimensions={0} | all-to-all | bytes 12582912 | tf_op jit(solution)/shard_map/all_to_all | solution.py:603
  147.4 6.2 %serve.3 = bf16[16,16,2048]{2,1,0:T(8,128)(2,1)} custom-call(bf16[16,96,2048]{2,1,0:T(8,128)(2,1)} %all_to_all.15.x_ref, bf16[1,2048,1024]{2,1,0:T(8,128)(2,1)S(1)} %copy-done.1, bf16[1,2048,1024]{2,1,0:T(8,128)(2,1)S(1)} %copy-done.2, bf16[1,1024,2048]{2,1,0:T(8,128)(2,1)S(1)} %copy-done.3), custom_call_target="tpu_custom_call" | custom-call | flops 2500000000 | bytes 5000000 | tf_op jit(solution)/shard_map/serve/pallas_call | solution.py:611
  153.5 3.7 %all-to-all-start.2 = ((bf16[16,16,2048]{2,1,0:T(8,128)(2,1)}), bf16[16,16,2048]{2,1,0:T(8,128)(2,1)S(1)}, u32[]{:S(2)}, u32[]{:S(2)}) async-start(bf16[16,16,2048]{2,1,0:T(8,128)(2,1)} %serve.3), calls=%async_computation.2 | async-start | bytes 2097152 | tf_op jit(solution)/shard_map/all_to_all | solution.py:603
  157.2 21.6 %serve.2 = bf16[16,80,2048]{2,1,0:T(8,128)(2,1)} custom-call(bf16[16,96,2048]{2,1,0:T(8,128)(2,1)} %all_to_all.15.x_ref, bf16[1,2048,1024]{2,1,0:T(8,128)(2,1)} %wg_ref.3, bf16[1,2048,1024]{2,1,0:T(8,128)(2,1)} %wu_ref.3, bf16[1,1024,2048]{2,1,0:T(8,128)(2,1)} %wd_ref.3), custom_call_target="tpu_custom_call" | custom-call | flops 10000000000 | bytes 20000000 | tf_op jit(solution)/shard_map/serve/pallas_call | solution.py:611
  179.8 7.2 %all-to-all-start.1 = ((bf16[16,80,2048]{2,1,0:T(8,128)(2,1)}), bf16[16,80,2048]{2,1,0:T(8,128)(2,1)}, u32[]{:S(2)}, u32[]{:S(2)}) async-start(bf16[16,80,2048]{2,1,0:T(8,128)(2,1)} %serve.2), calls=%async_computation.1 | async-start | bytes 10485760 | tf_op jit(solution)/shard_map/all_to_all | solution.py:603
  187.0 3.2 %weights.1 = (bf16[384,1280]{1,0:T(8,128)(2,1)}, bf16[384,256]{1,0:T(8,128)(2,1)}) custom-call(s32[8,384]{1,0:T(8,128)} %pad.8.routes_ref.refs_9_, f32[8,384]{1,0:T(8,128)} %pad.9.wt_ref), custom_call_target="tpu_custom_call" | custom-call | flops 1000000000 | bytes 2000000 | tf_op jit(solution)/shard_map/weights/pallas_call | solution.py:539
  190.2 72.6 %all-to-all-done.1 = bf16[16,80,2048]{2,1,0:T(8,128)(2,1)} async-done(((bf16[16,80,2048]{2,1,0:T(8,128)(2,1)}), bf16[16,80,2048]{2,1,0:T(8,128)(2,1)}, u32[]{:S(2)}, u32[]{:S(2)}) %all-to-all-start.1) | async-done | bytes 5242912 | tf_op jit(solution)/shard_map/all_to_all | solution.py:603
  262.8 1.2 copy-done.5
  264.0 1.4 copy-done.6
  265.4 1.2 copy-done.7
  267.5 5.9 %combine.1 = bf16[384,2048]{1,0:T(8,128)(2,1)} custom-call(bf16[384,1280]{1,0:T(8,128)(2,1)S(1)} %copy-done.7, bf16[384,256]{1,0:T(8,128)(2,1)S(1)} %copy-done.8, bf16[1280,2048]{1,0:T(8,128)(2,1)} %bitcast.19.got_ref, bf16[256,2048]{1,0:T(8,128)(2,1)S(1)} %bitcast.25, bf16[384,2048]{1,0:T(8,128)(2,1)S(1)} %copy-done.6), custom_call_target="tpu_custom_call" | custom-call | flops 2000000000 | bytes 4000000 | tf_op jit(solution)/shard_map/combine/pallas_call | solution.py:643
  (47 shorter events, 8.3 us)
Async XLA Ops:
  1.6 10.0 %copy-start.11 = (bf16[128,2048]{1,0:T(8,128)(2,1)S(1)}, bf16[128,2048]{1,0:T(8,128)(2,1)}, u32[]{:S(2)}) copy-start(bf16[128,2048]{1,0:T(8,128)(2,1)} %refs_0_.1) | copy-start | bytes 1572868
  8.4 8.2 %collective-permute-start.2 = (bf16[80,1024]{1,0:T(8,128)(2,1)}, bf16[80,1024]{1,0:T(8,128)(2,1)}, u32[]{:S(2)}, u32[]{:S(2)}) collective-permute-start(bf16[80,1024]{1,0:T(8,128)(2,1)} %states.1.own_ref), channel_id=1, source_target_pairs={{0,24},{8,0},{16,8},{24,16},{1,25},{9,1},{17,9},{25,17},{2,26},{10... | collective-permute-start | bytes 491528 | tf_op jit(solution)/shard_map/ppermute | solution.py:499
  11.6 24.9 %collective-permute-start.8 = (bf16[128,2048]{1,0:T(8,128)(2,1)S(1)}, bf16[128,2048]{1,0:T(8,128)(2,1)}, u32[]{:S(2)}, u32[]{:S(2)}) collective-permute-start(bf16[128,2048]{1,0:T(8,128)(2,1)S(1)} %copy-done.11), channel_id=1, source_target_pairs={{0,6},{2,0},{4,2},{6,4},{1,7},{3,1},{5,3},{7,5},{8,14},{10,8},{12,... | collective-permute-start | bytes 1572872 | tf_op jit(solution)/shard_map/ppermute | solution.py:483
  14.3 22.2 %collective-permute-start.7 = (bf16[128,2048]{1,0:T(8,128)(2,1)S(1)}, bf16[128,2048]{1,0:T(8,128)(2,1)}, u32[]{:S(2)}, u32[]{:S(2)}) collective-permute-start(bf16[128,2048]{1,0:T(8,128)(2,1)S(1)} %copy-done.11), channel_id=1, source_target_pairs={{0,4},{2,6},{4,0},{6,2},{1,5},{3,7},{5,1},{7,3},{8,12},{10,14},{12... | collective-permute-start | bytes 1572872 | tf_op jit(solution)/shard_map/ppermute | solution.py:483
  15.1 25.2 %collective-permute-start.6 = (bf16[128,2048]{1,0:T(8,128)(2,1)S(1)}, bf16[128,2048]{1,0:T(8,128)(2,1)}, u32[]{:S(2)}, u32[]{:S(2)}) collective-permute-start(bf16[128,2048]{1,0:T(8,128)(2,1)S(1)} %copy-done.11), channel_id=1, source_target_pairs={{0,2},{2,4},{4,6},{6,0},{1,3},{3,5},{5,7},{7,1},{8,10},{10,12},{12... | collective-permute-start | bytes 1572872 | tf_op jit(solution)/shard_map/ppermute | solution.py:483
  16.0 8.4 %collective-permute-start.1 = (bf16[80,1024]{1,0:T(8,128)(2,1)}, bf16[80,1024]{1,0:T(8,128)(2,1)}, u32[]{:S(2)}, u32[]{:S(2)}) collective-permute-start(bf16[80,1024]{1,0:T(8,128)(2,1)} %states.1.own_ref), channel_id=1, source_target_pairs={{0,16},{8,24},{16,0},{24,8},{1,17},{9,25},{17,1},{25,9},{2,18},{10... | collective-permute-start | bytes 491528 | tf_op jit(solution)/shard_map/ppermute | solution.py:499
  16.6 9.5 %collective-permute-start = (bf16[80,1024]{1,0:T(8,128)(2,1)}, bf16[80,1024]{1,0:T(8,128)(2,1)}, u32[]{:S(2)}, u32[]{:S(2)}) collective-permute-start(bf16[80,1024]{1,0:T(8,128)(2,1)} %states.1.own_ref), channel_id=1, source_target_pairs={{0,8},{8,16},{16,24},{24,0},{1,9},{9,17},{17,25},{25,1},{2,10},{10... | collective-permute-start | bytes 491528 | tf_op jit(solution)/shard_map/ppermute | solution.py:499
  28.3 12.5 %collective-permute-start.5 = (bf16[80,1024]{1,0:T(8,128)(2,1)}, bf16[80,1024]{1,0:T(8,128)(2,1)S(1)}, u32[]{:S(2)}, u32[]{:S(2)}) collective-permute-start(bf16[80,1024]{1,0:T(8,128)(2,1)} %get-tuple-element.27), channel_id=1, source_target_pairs={{0,96},{32,0},{64,32},{96,64},{1,97},{33,1},{65,33},{97,65},{2,98}... | collective-permute-start | bytes 491528 | tf_op jit(solution)/shard_map/ppermute | solution.py:530
  32.3 8.5 %collective-permute-start.4 = (bf16[80,1024]{1,0:T(8,128)(2,1)}, bf16[80,1024]{1,0:T(8,128)(2,1)S(1)}, u32[]{:S(2)}, u32[]{:S(2)}) collective-permute-start(bf16[80,1024]{1,0:T(8,128)(2,1)} %get-tuple-element.27), channel_id=1, source_target_pairs={{0,64},{32,96},{64,0},{96,32},{1,65},{33,97},{65,1},{97,33},{2,66}... | collective-permute-start | bytes 491528 | tf_op jit(solution)/shard_map/ppermute | solution.py:530
  36.5 16.4 %collective-permute-start.9 = (bf16[128,2048]{1,0:T(8,128)(2,1)S(1)}, bf16[128,2048]{1,0:T(8,128)(2,1)}, u32[]{:S(2)}, u32[]{:S(2)}) collective-permute-start(bf16[128,2048]{1,0:T(8,128)(2,1)S(1)} %copy-done.11), channel_id=1, source_target_pairs={{0,1},{1,0},{2,3},{3,2},{4,5},{5,4},{6,7},{7,6},{8,9},{9,8},{10,11... | collective-permute-start | bytes 1572872 | tf_op jit(solution)/shard_map/ppermute | solution.py:534
  40.3 12.7 %collective-permute-start.10 = (bf16[128,2048]{1,0:T(8,128)(2,1)}, bf16[128,2048]{1,0:T(8,128)(2,1)}, u32[]{:S(2)}, u32[]{:S(2)}) collective-permute-start(bf16[128,2048]{1,0:T(8,128)(2,1)} %collective-permute-done.6.refs_1_), channel_id=1, source_target_pairs={{0,1},{1,0},{2,3},{3,2},{4,5},{5,4},{6,7},{7,6},{8,9},{9,8},{10,11... | collective-permute-start | bytes 1572872 | tf_op jit(solution)/shard_map/ppermute | solution.py:534
  40.3 12.6 %collective-permute-start.11 = (bf16[128,2048]{1,0:T(8,128)(2,1)}, bf16[128,2048]{1,0:T(8,128)(2,1)}, u32[]{:S(2)}, u32[]{:S(2)}) collective-permute-start(bf16[128,2048]{1,0:T(8,128)(2,1)} %collective-permute-done.7.refs_2_), channel_id=1, source_target_pairs={{0,1},{1,0},{2,3},{3,2},{4,5},{5,4},{6,7},{7,6},{8,9},{9,8},{10,11... | collective-permute-start | bytes 1572872 | tf_op jit(solution)/shard_map/ppermute | solution.py:534
  40.8 2.0 copy-start.12
  40.8 12.2 %collective-permute-start.12 = (bf16[128,2048]{1,0:T(8,128)(2,1)}, bf16[128,2048]{1,0:T(8,128)(2,1)}, u32[]{:S(2)}, u32[]{:S(2)}) collective-permute-start(bf16[128,2048]{1,0:T(8,128)(2,1)} %collective-permute-done.8.refs_3_), channel_id=1, source_target_pairs={{0,1},{1,0},{2,3},{3,2},{4,5},{5,4},{6,7},{7,6},{8,9},{9,8},{10,11... | collective-permute-start | bytes 1572872 | tf_op jit(solution)/shard_map/ppermute | solution.py:534
  40.9 1.9 copy-start.13
  40.9 12.0 %collective-permute-start.3 = (bf16[80,1024]{1,0:T(8,128)(2,1)}, bf16[80,1024]{1,0:T(8,128)(2,1)}, u32[]{:S(2)}, u32[]{:S(2)}) collective-permute-start(bf16[80,1024]{1,0:T(8,128)(2,1)} %get-tuple-element.27), channel_id=1, source_target_pairs={{0,32},{32,64},{64,96},{96,0},{1,33},{33,65},{65,97},{97,1},{2,34}... | collective-permute-start | bytes 491528 | tf_op jit(solution)/shard_map/ppermute | solution.py:530
  42.8 8.3 %copy-start.9 = (s32[1,384,2]{1,2,0:T(2,128)S(1)}, s32[1,384,2]{1,2,0:T(2,128)}, u32[]{:S(2)}) copy-start(s32[1,384,2]{1,2,0:T(2,128)} %param.26) | copy-start | bytes 9220
  42.8 8.9 %copy-start.10 = (f32[1,384,2]{1,2,0:T(2,128)S(1)}, f32[1,384,2]{1,2,0:T(2,128)}, u32[]{:S(2)}) copy-start(f32[1,384,2]{1,2,0:T(2,128)} %param.27) | copy-start | bytes 9220
  67.1 80.3 %copy-start.1 = (bf16[1,2048,1024]{2,1,0:T(8,128)(2,1)S(1)}, bf16[1,2048,1024]{2,1,0:T(8,128)(2,1)}, u32[]{:S(2)}) copy-start(bf16[1,2048,1024]{2,1,0:T(8,128)(2,1)} %wg_ref.3) | copy-start | bytes 12582916
  67.1 80.2 %copy-start.2 = (bf16[1,2048,1024]{2,1,0:T(8,128)(2,1)S(1)}, bf16[1,2048,1024]{2,1,0:T(8,128)(2,1)}, u32[]{:S(2)}) copy-start(bf16[1,2048,1024]{2,1,0:T(8,128)(2,1)} %wu_ref.3) | copy-start | bytes 12582916
  67.1 80.2 %copy-start.3 = (bf16[1,1024,2048]{2,1,0:T(8,128)(2,1)S(1)}, bf16[1,1024,2048]{2,1,0:T(8,128)(2,1)}, u32[]{:S(2)}) copy-start(bf16[1,1024,2048]{2,1,0:T(8,128)(2,1)} %wd_ref.3) | copy-start | bytes 12582916
  153.5 25.3 %all-to-all-start.2 = ((bf16[16,16,2048]{2,1,0:T(8,128)(2,1)}), bf16[16,16,2048]{2,1,0:T(8,128)(2,1)S(1)}, u32[]{:S(2)}, u32[]{:S(2)}) async-start(bf16[16,16,2048]{2,1,0:T(8,128)(2,1)} %serve.3), calls=%async_computation.2 | async-start | bytes 2097152 | tf_op jit(solution)/shard_map/all_to_all | solution.py:603
  179.8 83.0 %all-to-all-start.1 = ((bf16[16,80,2048]{2,1,0:T(8,128)(2,1)}), bf16[16,80,2048]{2,1,0:T(8,128)(2,1)}, u32[]{:S(2)}, u32[]{:S(2)}) async-start(bf16[16,80,2048]{2,1,0:T(8,128)(2,1)} %serve.2), calls=%async_computation.1 | async-start | bytes 10485760 | tf_op jit(solution)/shard_map/all_to_all | solution.py:603
  264.0 1.4 copy-start.6
  (5 other events, 5.3 us)

commit v3 on v2

--- a/solution.py
+++ b/solution.py
@@ -55,8 +55,8 @@
 def keys_and_logs(f_ref, floor_ref, spike_ref, group):
     f = f_ref[...].astype(F32)
     keys = (1.0 - floor_ref[...]) / (1.0 + jnp.exp(f))
-    poly = jnp.full_like(keys, 1.0 / 10.0)
-    for n in range(9, 0, -1):
+    poly = jnp.full_like(keys, 1.0 / 7.0)
+    for n in range(6, 0, -1):
         poly = poly * keys + 1.0 / n
     heads = spike_ref.shape[0]
     spread = (
@@ -73,8 +73,8 @@
     lower = tri(length).astype(BF)
     out = []
     for b in range(logs.shape[0] // length):
-        hi, mid, low = split3(logs[b * length : (b + 1) * length])
-        out.append(dot(lower, hi) + dot(lower, mid) + dot(lower, low))
+        hi, low = split2(logs[b * length : (b + 1) * length])
+        out.append(dot(lower, hi) + dot(lower, low))
     return out
 
 
@@ -120,7 +120,8 @@
         qd = q[rows] * jnp.exp(cum)
         qrun_ref[rows, :] = (qd * jnp.exp(before)).astype(BF)
         qd = qd.astype(BF)
-        kg = (k * grow).astype(BF)
+        k = k * grow
+        kg = k.astype(BF)
         v = v_ref[rows, :]
         k4 = jnp.where(head_mask, jnp.concatenate([kg] * 4, axis=0), zero)
         v4 = jnp.where(head_mask, jnp.concatenate([v] * 4, axis=0), zero)
@@ -131,7 +132,7 @@
             out = out + dot(qd, state.astype(BF), ((1,), (1,)))
         out_ref[rows, :] = out
         if b + 1 < len(parts):
-            kc = (k * jnp.exp(close - cum)).astype(BF)
+            kc = (k * jnp.exp(close)).astype(BF)
             add = jnp.where(head_mask, dot(v, kc, ((0,), (0,))), 0.0)
             state = jnp.exp(close) * state + add
         before = before + close
@@ -551,7 +552,7 @@
 
 
     place = jnp.stack([z, x, core]).astype(jnp.int32)
-    tok_steps = 3
+    tok_steps = 2
     rows = tok // tok_steps
     send_steps = 4
     send_rows = experts * cap // send_steps

time: 274 us -> 273 us (level)
  no operation moved by 1% of the time
where the time goes in v3:
time: 273 us
  waiting for transfers between devices  89.1 us (33%)
  blocking collectives  80.2 us (29%)
  Pallas kernels  67.3 us (25%)
  starting transfers between devices  26.6 us (10%)
  local copies, waits for them, and re-layouts  8.57 us (3%)
    all_to_all x1, blocking collectives, exchange(): return lax.all_to_all(a, SP, split_axis=0, concat_axis=0, tiled=True)  80.2 us
    all_to_all x2, waiting for transfers between devices, exchange(): return lax.all_to_all(a, SP, split_axis=0, concat_axis=0, tiled=True)  72.6 us
    pallas_call x2, Pallas kernels, serve(): pl.pallas_call(functools.partial(kernel, first, parts), in_specs=[anywher...  27.7 us
    pallas_call x1, Pallas kernels, per_device(): pl.pallas_call(functools.partial(mix_kernel, tok_steps, cap), grid=(tok_s...  13.7 us
    all_to_all x2, starting transfers between devices, exchange(): return lax.all_to_all(a, SP, split_axis=0, concat_axis=0, tiled=True)  10.8 us
    ppermute x3, waiting for transfers between devices, per_device(): along_y = [lax.ppermute(pack, 'sp_1', ring(n)) for n in (1, 2, 3)]  8.55 us
    pallas_call x1, Pallas kernels, per_device(): pl.pallas_call(inside_kernel, grid=(groups,), in_specs=[tall, tall, tall,...  8.29 us
    ppermute x3, waiting for transfers between devices, per_device(): wmine = [lax.ppermute(mine, 'x', ring(n)) for n in (1, 2, 3)]  7.92 us
  transfers between devices with their start and end apart: 15, of which 5 were waited for; matrix products, arithmetic and copies ran while one was open for 1% of the time, Pallas kernels for 13%

profile of v3, /device:TPU:0, one launch (start us, length us, event | category | flops | bytes accessed | tf_op | source)
XLA Modules:
  0.0 272.7 jit_solution(16615806577885413807)
XLA Ops:
  0.0 1.0 copy-done
  1.6 6.3 %states.1.own_ref = bf16[80,1024]{1,0:T(8,128)(2,1)} custom-call(bf16[384,1024]{1,0:T(8,128)(2,1)} %bitcast.31, bf16[384,1024]{1,0:T(8,128)(2,1)} %bitcast.33, f32[1,1024]{1,0:T(1,128)} %bitcast.37, f32[16,384]{1,0:T(8,128)} %dynamic-slice_bitcast_fusion.spike_ref), custom_call_target="tpu_custom_call" | custom-call | flops 3500000000 | bytes 7000000 | tf_op jit(solution)/shard_map/states/pallas_call | solution.py:489
  7.9 3.1 %collective-permute-start.2 = (bf16[80,1024]{1,0:T(8,128)(2,1)}, bf16[80,1024]{1,0:T(8,128)(2,1)}, u32[]{:S(2)}, u32[]{:S(2)}) collective-permute-start(bf16[80,1024]{1,0:T(8,128)(2,1)} %states.1.own_ref), channel_id=1, source_target_pairs={{0,24},{8,0},{16,8},{24,16},{1,25},{9,1},{17,9},{25,17},{2,26},{10... | collective-permute-start | bytes 491528 | tf_op jit(solution)/shard_map/ppermute | solution.py:500
  11.1 2.8 %collective-permute-start.8 = (bf16[128,2048]{1,0:T(8,128)(2,1)S(1)}, bf16[128,2048]{1,0:T(8,128)(2,1)}, u32[]{:S(2)}, u32[]{:S(2)}) collective-permute-start(bf16[128,2048]{1,0:T(8,128)(2,1)S(1)} %copy-done.11), channel_id=1, source_target_pairs={{0,6},{2,0},{4,2},{6,4},{1,7},{3,1},{5,3},{7,5},{8,14},{10,8},{12,... | collective-permute-start | bytes 1572872 | tf_op jit(solution)/shard_map/ppermute | solution.py:484
  17.1 6.8 %collective-permute-done.1.two_ref = bf16[80,1024]{1,0:T(8,128)(2,1)} collective-permute-done((bf16[80,1024]{1,0:T(8,128)(2,1)}, bf16[80,1024]{1,0:T(8,128)(2,1)}, u32[]{:S(2)}, u32[]{:S(2)}) %collective-permute-start.1) | collective-permute-done | bytes 163872 | tf_op jit(solution)/shard_map/ppermute | solution.py:500
  23.9 1.7 collective-permute-done.one_ref
  25.7 2.1 row.1
  27.8 4.0 %collective-permute-start.5 = (bf16[80,1024]{1,0:T(8,128)(2,1)}, bf16[80,1024]{1,0:T(8,128)(2,1)S(1)}, u32[]{:S(2)}, u32[]{:S(2)}) collective-permute-start(bf16[80,1024]{1,0:T(8,128)(2,1)} %get-tuple-element.27), channel_id=1, source_target_pairs={{0,96},{32,0},{64,32},{96,64},{1,97},{33,1},{65,33},{97,65},{2,98}... | collective-permute-start | bytes 491528 | tf_op jit(solution)/shard_map/ppermute | solution.py:531
  31.8 4.1 %collective-permute-done.8.refs_3_ = bf16[128,2048]{1,0:T(8,128)(2,1)} collective-permute-done((bf16[128,2048]{1,0:T(8,128)(2,1)S(1)}, bf16[128,2048]{1,0:T(8,128)(2,1)}, u32[]{:S(2)}, u32[]{:S(2)}) %collective-permute-start.8) | collective-permute-done | bytes 524320 | tf_op jit(solution)/shard_map/ppermute | solution.py:484
  36.0 3.8 %collective-permute-done.6.refs_1_ = bf16[128,2048]{1,0:T(8,128)(2,1)} collective-permute-done((bf16[128,2048]{1,0:T(8,128)(2,1)S(1)}, bf16[128,2048]{1,0:T(8,128)(2,1)}, u32[]{:S(2)}, u32[]{:S(2)}) %collective-permute-start.6) | collective-permute-done | bytes 524320 | tf_op jit(solution)/shard_map/ppermute | solution.py:484
  40.4 1.9 collective-permute-start.3
  42.3 8.3 %inside.1 = (f32[384,1024]{1,0:T(8,128)}, bf16[384,1024]{1,0:T(8,128)(2,1)}) custom-call(bf16[384,1024]{1,0:T(8,128)(2,1)} %bitcast.30, bf16[384,1024]{1,0:T(8,128)(2,1)} %bitcast.32, bf16[384,1024]{1,0:T(8,128)(2,1)} %bitcast.34, f32[1,1024]{1,0:T(1,128)} %bitcast.38, f32[16,384]{1,0:T(8,128)} %dynamic-slice_bitcast_fusion.spike_ref), custom_call_target="tpu_custom_call" | custom-call | flops 4000000000 | bytes 8000000 | tf_op jit(solution)/shard_map/inside/pallas_call | solution.py:506
  52.5 13.7 %mix.1 = (bf16[384,2048]{1,0:T(8,128)(2,1)}, bf16[1536,2048]{1,0:T(8,128)(2,1)}) custom-call(s32[3]{0:T(128)} %pad_add_fusion.pos_ref, f32[384,1024]{1,0:T(8,128)} %get-tuple-element.23.out_ref, bf16[384,1024]{1,0:T(8,128)(2,1)} %get-tuple-element.24.qrun_ref, bf16[384,1024]{1,0:T(8,128)(2,1)} %bitcast.35, bf16[384,2048]{1,0:T(8,128)(2,1)} %bitcast.29, ...), custom_call_target="tpu_custom_call" | custom-call | flops 6000000000 | bytes 12000000 | tf_op jit(solution)/shard_map/mix/pallas_call | solution.py:565
  66.2 80.2 %all_to_all.15.x_ref = bf16[16,96,2048]{2,1,0:T(8,128)(2,1)} all-to-all(bf16[16,96,2048]{2,1,0:T(8,128)(2,1)} %bitcast.26), channel_id=1, replica_groups=mesh['sp_0'=4,'sp_1'=4,'x'=4,'c'=2] {'sp_0','sp_1'}, dimensions={0} | all-to-all | bytes 12582912 | tf_op jit(solution)/shard_map/all_to_all | solution.py:604
  146.4 6.2 %serve.3 = bf16[16,16,2048]{2,1,0:T(8,128)(2,1)} custom-call(bf16[16,96,2048]{2,1,0:T(8,128)(2,1)} %all_to_all.15.x_ref, bf16[1,2048,1024]{2,1,0:T(8,128)(2,1)S(1)} %copy-done.1, bf16[1,2048,1024]{2,1,0:T(8,128)(2,1)S(1)} %copy-done.2, bf16[1,1024,2048]{2,1,0:T(8,128)(2,1)S(1)} %copy-done.3), custom_call_target="tpu_custom_call" | custom-call | flops 2500000000 | bytes 5000000 | tf_op jit(solution)/shard_map/serve/pallas_call | solution.py:612
  152.6 3.7 %all-to-all-start.2 = ((bf16[16,16,2048]{2,1,0:T(8,128)(2,1)}), bf16[16,16,2048]{2,1,0:T(8,128)(2,1)S(1)}, u32[]{:S(2)}, u32[]{:S(2)}) async-start(bf16[16,16,2048]{2,1,0:T(8,128)(2,1)} %serve.3), calls=%async_computation.2 | async-start | bytes 2097152 | tf_op jit(solution)/shard_map/all_to_all | solution.py:604
  156.3 21.6 %serve.2 = bf16[16,80,2048]{2,1,0:T(8,128)(2,1)} custom-call(bf16[16,96,2048]{2,1,0:T(8,128)(2,1)} %all_to_all.15.x_ref, bf16[1,2048,1024]{2,1,0:T(8,128)(2,1)} %wg_ref.3, bf16[1,2048,1024]{2,1,0:T(8,128)(2,1)} %wu_ref.3, bf16[1,1024,2048]{2,1,0:T(8,128)(2,1)} %wd_ref.3), custom_call_target="tpu_custom_call" | custom-call | flops 10000000000 | bytes 20000000 | tf_op jit(solution)/shard_map/serve/pallas_call | solution.py:612
  178.9 7.2 %all-to-all-start.1 = ((bf16[16,80,2048]{2,1,0:T(8,128)(2,1)}), bf16[16,80,2048]{2,1,0:T(8,128)(2,1)}, u32[]{:S(2)}, u32[]{:S(2)}) async-start(bf16[16,80,2048]{2,1,0:T(8,128)(2,1)} %serve.2), calls=%async_computation.1 | async-start | bytes 10485760 | tf_op jit(solution)/shard_map/all_to_all | solution.py:604
  186.1 3.2 %weights.1 = (bf16[384,1280]{1,0:T(8,128)(2,1)}, bf16[384,256]{1,0:T(8,128)(2,1)}) custom-call(s32[8,384]{1,0:T(8,128)} %pad.8.routes_ref.refs_9_, f32[8,384]{1,0:T(8,128)} %pad.9.wt_ref), custom_call_target="tpu_custom_call" | custom-call | flops 1000000000 | bytes 2000000 | tf_op jit(solution)/shard_map/weights/pallas_call | solution.py:540
  189.2 72.6 %all-to-all-done.1 = bf16[16,80,2048]{2,1,0:T(8,128)(2,1)} async-done(((bf16[16,80,2048]{2,1,0:T(8,128)(2,1)}), bf16[16,80,2048]{2,1,0:T(8,128)(2,1)}, u32[]{:S(2)}, u32[]{:S(2)}) %all-to-all-start.1) | async-done | bytes 5242912 | tf_op jit(solution)/shard_map/all_to_all | solution.py:604
  261.9 1.2 copy-done.5
  263.1 1.4 copy-done.6
  264.5 1.2 copy-done.7
  266.7 5.9 %combine.1 = bf16[384,2048]{1,0:T(8,128)(2,1)} custom-call(bf16[384,1280]{1,0:T(8,128)(2,1)S(1)} %copy-done.7, bf16[384,256]{1,0:T(8,128)(2,1)S(1)} %copy-done.8, bf16[1280,2048]{1,0:T(8,128)(2,1)} %bitcast.19.got_ref, bf16[256,2048]{1,0:T(8,128)(2,1)S(1)} %bitcast.25, bf16[384,2048]{1,0:T(8,128)(2,1)S(1)} %copy-done.6), custom_call_target="tpu_custom_call" | custom-call | flops 2000000000 | bytes 4000000 | tf_op jit(solution)/shard_map/combine/pallas_call | solution.py:644
  (47 shorter events, 8.3 us)
Async XLA Ops:
  1.6 9.5 %copy-start.11 = (bf16[128,2048]{1,0:T(8,128)(2,1)S(1)}, bf16[128,2048]{1,0:T(8,128)(2,1)}, u32[]{:S(2)}) copy-start(bf16[128,2048]{1,0:T(8,128)(2,1)} %refs_0_.1) | copy-start | bytes 1572868
  7.9 8.2 %collective-permute-start.2 = (bf16[80,1024]{1,0:T(8,128)(2,1)}, bf16[80,1024]{1,0:T(8,128)(2,1)}, u32[]{:S(2)}, u32[]{:S(2)}) collective-permute-start(bf16[80,1024]{1,0:T(8,128)(2,1)} %states.1.own_ref), channel_id=1, source_target_pairs={{0,24},{8,0},{16,8},{24,16},{1,25},{9,1},{17,9},{25,17},{2,26},{10... | collective-permute-start | bytes 491528 | tf_op jit(solution)/shard_map/ppermute | solution.py:500
  11.1 24.9 %collective-permute-start.8 = (bf16[128,2048]{1,0:T(8,128)(2,1)S(1)}, bf16[128,2048]{1,0:T(8,128)(2,1)}, u32[]{:S(2)}, u32[]{:S(2)}) collective-permute-start(bf16[128,2048]{1,0:T(8,128)(2,1)S(1)} %copy-done.11), channel_id=1, source_target_pairs={{0,6},{2,0},{4,2},{6,4},{1,7},{3,1},{5,3},{7,5},{8,14},{10,8},{12,... | collective-permute-start | bytes 1572872 | tf_op jit(solution)/shard_map/ppermute | solution.py:484
  13.8 22.2 %collective-permute-start.7 = (bf16[128,2048]{1,0:T(8,128)(2,1)S(1)}, bf16[128,2048]{1,0:T(8,128)(2,1)}, u32[]{:S(2)}, u32[]{:S(2)}) collective-permute-start(bf16[128,2048]{1,0:T(8,128)(2,1)S(1)} %copy-done.11), channel_id=1, source_target_pairs={{0,4},{2,6},{4,0},{6,2},{1,5},{3,7},{5,1},{7,3},{8,12},{10,14},{12... | collective-permute-start | bytes 1572872 | tf_op jit(solution)/shard_map/ppermute | solution.py:484
  14.6 25.1 %collective-permute-start.6 = (bf16[128,2048]{1,0:T(8,128)(2,1)S(1)}, bf16[128,2048]{1,0:T(8,128)(2,1)}, u32[]{:S(2)}, u32[]{:S(2)}) collective-permute-start(bf16[128,2048]{1,0:T(8,128)(2,1)S(1)} %copy-done.11), channel_id=1, source_target_pairs={{0,2},{2,4},{4,6},{6,0},{1,3},{3,5},{5,7},{7,1},{8,10},{10,12},{12... | collective-permute-start | bytes 1572872 | tf_op jit(solution)/shard_map/ppermute | solution.py:484
  15.5 8.4 %collective-permute-start.1 = (bf16[80,1024]{1,0:T(8,128)(2,1)}, bf16[80,1024]{1,0:T(8,128)(2,1)}, u32[]{:S(2)}, u32[]{:S(2)}) collective-permute-start(bf16[80,1024]{1,0:T(8,128)(2,1)} %states.1.own_ref), channel_id=1, source_target_pairs={{0,16},{8,24},{16,0},{24,8},{1,17},{9,25},{17,1},{25,9},{2,18},{10... | collective-permute-start | bytes 491528 | tf_op jit(solution)/shard_map/ppermute | solution.py:500
  16.1 9.5 %collective-permute-start = (bf16[80,1024]{1,0:T(8,128)(2,1)}, bf16[80,1024]{1,0:T(8,128)(2,1)}, u32[]{:S(2)}, u32[]{:S(2)}) collective-permute-start(bf16[80,1024]{1,0:T(8,128)(2,1)} %states.1.own_ref), channel_id=1, source_target_pairs={{0,8},{8,16},{16,24},{24,0},{1,9},{9,17},{17,25},{25,1},{2,10},{10... | collective-permute-start | bytes 491528 | tf_op jit(solution)/shard_map/ppermute | solution.py:500
  27.8 12.5 %collective-permute-start.5 = (bf16[80,1024]{1,0:T(8,128)(2,1)}, bf16[80,1024]{1,0:T(8,128)(2,1)S(1)}, u32[]{:S(2)}, u32[]{:S(2)}) collective-permute-start(bf16[80,1024]{1,0:T(8,128)(2,1)} %get-tuple-element.27), channel_id=1, source_target_pairs={{0,96},{32,0},{64,32},{96,64},{1,97},{33,1},{65,33},{97,65},{2,98}... | collective-permute-start | bytes 491528 | tf_op jit(solution)/shard_map/ppermute | solution.py:531
  31.8 8.5 %collective-permute-start.4 = (bf16[80,1024]{1,0:T(8,128)(2,1)}, bf16[80,1024]{1,0:T(8,128)(2,1)S(1)}, u32[]{:S(2)}, u32[]{:S(2)}) collective-permute-start(bf16[80,1024]{1,0:T(8,128)(2,1)} %get-tuple-element.27), channel_id=1, source_target_pairs={{0,64},{32,96},{64,0},{96,32},{1,65},{33,97},{65,1},{97,33},{2,66}... | collective-permute-start | bytes 491528 | tf_op jit(solution)/shard_map/ppermute | solution.py:531
  36.0 16.5 %collective-permute-start.9 = (bf16[128,2048]{1,0:T(8,128)(2,1)S(1)}, bf16[128,2048]{1,0:T(8,128)(2,1)}, u32[]{:S(2)}, u32[]{:S(2)}) collective-permute-start(bf16[128,2048]{1,0:T(8,128)(2,1)S(1)} %copy-done.11), channel_id=1, source_target_pairs={{0,1},{1,0},{2,3},{3,2},{4,5},{5,4},{6,7},{7,6},{8,9},{9,8},{10,11... | collective-permute-start | bytes 1572872 | tf_op jit(solution)/shard_map/ppermute | solution.py:535
  39.8 12.7 %collective-permute-start.10 = (bf16[128,2048]{1,0:T(8,128)(2,1)}, bf16[128,2048]{1,0:T(8,128)(2,1)}, u32[]{:S(2)}, u32[]{:S(2)}) collective-permute-start(bf16[128,2048]{1,0:T(8,128)(2,1)} %collective-permute-done.6.refs_1_), channel_id=1, source_target_pairs={{0,1},{1,0},{2,3},{3,2},{4,5},{5,4},{6,7},{7,6},{8,9},{9,8},{10,11... | collective-permute-start | bytes 1572872 | tf_op jit(solution)/shard_map/ppermute | solution.py:535
  39.8 12.7 %collective-permute-start.11 = (bf16[128,2048]{1,0:T(8,128)(2,1)}, bf16[128,2048]{1,0:T(8,128)(2,1)}, u32[]{:S(2)}, u32[]{:S(2)}) collective-permute-start(bf16[128,2048]{1,0:T(8,128)(2,1)} %collective-permute-done.7.refs_2_), channel_id=1, source_target_pairs={{0,1},{1,0},{2,3},{3,2},{4,5},{5,4},{6,7},{7,6},{8,9},{9,8},{10,11... | collective-permute-start | bytes 1572872 | tf_op jit(solution)/shard_map/ppermute | solution.py:535
  40.3 2.0 copy-start.12
  40.3 12.2 %collective-permute-start.12 = (bf16[128,2048]{1,0:T(8,128)(2,1)}, bf16[128,2048]{1,0:T(8,128)(2,1)}, u32[]{:S(2)}, u32[]{:S(2)}) collective-permute-start(bf16[128,2048]{1,0:T(8,128)(2,1)} %collective-permute-done.8.refs_3_), channel_id=1, source_target_pairs={{0,1},{1,0},{2,3},{3,2},{4,5},{5,4},{6,7},{7,6},{8,9},{9,8},{10,11... | collective-permute-start | bytes 1572872 | tf_op jit(solution)/shard_map/ppermute | solution.py:535
  40.4 1.9 copy-start.13
  40.4 12.1 %collective-permute-start.3 = (bf16[80,1024]{1,0:T(8,128)(2,1)}, bf16[80,1024]{1,0:T(8,128)(2,1)}, u32[]{:S(2)}, u32[]{:S(2)}) collective-permute-start(bf16[80,1024]{1,0:T(8,128)(2,1)} %get-tuple-element.27), channel_id=1, source_target_pairs={{0,32},{32,64},{64,96},{96,0},{1,33},{33,65},{65,97},{97,1},{2,34}... | collective-permute-start | bytes 491528 | tf_op jit(solution)/shard_map/ppermute | solution.py:531
  42.3 8.3 %copy-start.9 = (s32[1,384,2]{1,2,0:T(2,128)S(1)}, s32[1,384,2]{1,2,0:T(2,128)}, u32[]{:S(2)}) copy-start(s32[1,384,2]{1,2,0:T(2,128)} %param.26) | copy-start | bytes 9220
  42.3 8.9 %copy-start.10 = (f32[1,384,2]{1,2,0:T(2,128)S(1)}, f32[1,384,2]{1,2,0:T(2,128)}, u32[]{:S(2)}) copy-start(f32[1,384,2]{1,2,0:T(2,128)} %param.27) | copy-start | bytes 9220
  66.2 80.3 %copy-start.1 = (bf16[1,2048,1024]{2,1,0:T(8,128)(2,1)S(1)}, bf16[1,2048,1024]{2,1,0:T(8,128)(2,1)}, u32[]{:S(2)}) copy-start(bf16[1,2048,1024]{2,1,0:T(8,128)(2,1)} %wg_ref.3) | copy-start | bytes 12582916
  66.2 80.2 %copy-start.2 = (bf16[1,2048,1024]{2,1,0:T(8,128)(2,1)S(1)}, bf16[1,2048,1024]{2,1,0:T(8,128)(2,1)}, u32[]{:S(2)}) copy-start(bf16[1,2048,1024]{2,1,0:T(8,128)(2,1)} %wu_ref.3) | copy-start | bytes 12582916
  66.2 80.2 %copy-start.3 = (bf16[1,1024,2048]{2,1,0:T(8,128)(2,1)S(1)}, bf16[1,1024,2048]{2,1,0:T(8,128)(2,1)}, u32[]{:S(2)}) copy-start(bf16[1,1024,2048]{2,1,0:T(8,128)(2,1)} %wd_ref.3) | copy-start | bytes 12582916
  152.6 25.3 %all-to-all-start.2 = ((bf16[16,16,2048]{2,1,0:T(8,128)(2,1)}), bf16[16,16,2048]{2,1,0:T(8,128)(2,1)S(1)}, u32[]{:S(2)}, u32[]{:S(2)}) async-start(bf16[16,16,2048]{2,1,0:T(8,128)(2,1)} %serve.3), calls=%async_computation.2 | async-start | bytes 2097152 | tf_op jit(solution)/shard_map/all_to_all | solution.py:604
  178.9 83.0 %all-to-all-start.1 = ((bf16[16,80,2048]{2,1,0:T(8,128)(2,1)}), bf16[16,80,2048]{2,1,0:T(8,128)(2,1)}, u32[]{:S(2)}, u32[]{:S(2)}) async-start(bf16[16,80,2048]{2,1,0:T(8,128)(2,1)} %serve.2), calls=%async_computation.1 | async-start | bytes 10485760 | tf_op jit(solution)/shard_map/all_to_all | solution.py:604
  263.1 1.4 copy-start.6
  (5 other events, 5.3 us)

commit v4 on v3

--- a/solution.py
+++ b/solution.py
@@ -13,7 +13,7 @@
 GL = 256
 SP = ("sp_0", "sp_1")
 DP = ("x", "c")
-PACK = 80
+PACK = 72
 F32 = jnp.float32
 BF = jnp.bfloat16
 
@@ -93,11 +93,11 @@
     compact = acc[0:64] + acc[64:128] + acc[128:192] + acc[192:256]
     pack_ref[0:64, :] = compact.astype(BF)
     hi, mid, low = split3(after)
-    row = lax.broadcasted_iota(jnp.int32, (16, GL), 0)
+    row = lax.broadcasted_iota(jnp.int32, (8, GL), 0)
     tail = jnp.where(row == 0, hi.astype(F32), 0.0)
     tail = jnp.where(row == 1, mid.astype(F32), tail)
     tail = jnp.where(row == 2, low.astype(F32), tail)
-    pack_ref[64:80, :] = tail.astype(BF)
+    pack_ref[64:72, :] = tail.astype(BF)
 
 
 def inside_kernel(q_ref, f_ref, v_ref, floor_ref, spike_ref, out_ref, qrun_ref):
@@ -169,11 +169,11 @@
         total = total + t
     row_ref[0:64, :] = state.astype(BF)
     hi, mid, low = split3(total)
-    row = lax.broadcasted_iota(jnp.int32, (16, width), 0)
+    row = lax.broadcasted_iota(jnp.int32, (8, width), 0)
     tail = jnp.where(row == 0, hi.astype(F32), 0.0)
     tail = jnp.where(row == 1, mid.astype(F32), tail)
     tail = jnp.where(row == 2, low.astype(F32), tail)
-    row_ref[64:80, :] = tail.astype(BF)
+    row_ref[64:72, :] = tail.astype(BF)
 
 
 def mix_kernel(
@@ -528,7 +528,7 @@
         name="row",
     )(y.astype(jnp.int32).reshape(1), pack, *along_y)
 
-    along_z = [lax.ppermute(row, "sp_0", ring(n)) for n in (1, 2, 3)]
+    along_z = [lax.ppermute(row, "sp_0", ring(n)[: 4 - n]) for n in (1, 2, 3)]
 
     wmine, row = lax.optimization_barrier((wmine, row))
     wmine = [mine] + wmine

time: 273 us -> 276 us (1.011)
  starting transfers between devices: 26.6 us -> 32.3 us
  waiting for transfers between devices: 89.1 us -> 86 us
    ppermute x3, starting transfers between devices: 5.96 us -> 11.7 us  [per_device(): along_z = [lax.ppermute(row, 'sp_0', ring(n)[:4 - n]) for n in (1, 2, 3)]]
where the time goes in v4:
time: 276 us; the launch traced here: 275 us
  waiting for transfers between devices  86 us (31%)
  blocking collectives  80.2 us (29%)
  Pallas kernels  67.2 us (24%)
  starting transfers between devices  32.3 us (12%)
  local copies, waits for them, and re-layouts  8.57 us (3%)
    all_to_all x1, blocking collectives, exchange(): return lax.all_to_all(a, SP, split_axis=0, concat_axis=0, tiled=True)  80.2 us
    all_to_all x2, waiting for transfers between devices, exchange(): return lax.all_to_all(a, SP, split_axis=0, concat_axis=0, tiled=True)  72.7 us
    pallas_call x2, Pallas kernels, serve(): pl.pallas_call(functools.partial(kernel, first, parts), in_specs=[anywher...  27.7 us
    pallas_call x1, Pallas kernels, per_device(): pl.pallas_call(functools.partial(mix_kernel, tok_steps, cap), grid=(tok_s...  13.7 us
    ppermute x3, starting transfers between devices, per_device(): along_z = [lax.ppermute(row, 'sp_0', ring(n)[:4 - n]) for n in (1, 2, 3)]  11.7 us
    all_to_all x2, starting transfers between devices, exchange(): return lax.all_to_all(a, SP, split_axis=0, concat_axis=0, tiled=True)  10.8 us
    pallas_call x1, Pallas kernels, per_device(): pl.pallas_call(inside_kernel, grid=(groups,), in_specs=[tall, tall, tall,...  8.29 us
    ppermute x3, waiting for transfers between devices, per_device(): along_y = [lax.ppermute(pack, 'sp_1', ring(n)) for n in (1, 2, 3)]  7.85 us
  transfers between devices with their start and end apart: 15, of which 5 were waited for; matrix products, arithmetic and copies ran while one was open for 1% of the time, Pallas kernels for 13%

profile of v4, /device:TPU:0, one launch (start us, length us, event | category | flops | bytes accessed | tf_op | source)
XLA Modules:
  0.0 275.3 jit_solution(3206612112861103286)
XLA Ops:
  1.6 6.3 %states.1.own_ref = bf16[72,1024]{1,0:T(8,128)(2,1)} custom-call(bf16[384,1024]{1,0:T(8,128)(2,1)} %bitcast.31, bf16[384,1024]{1,0:T(8,128)(2,1)} %bitcast.33, f32[1,1024]{1,0:T(1,128)} %bitcast.37, f32[16,384]{1,0:T(8,128)} %dynamic-slice_bitcast_fusion.spike_ref), custom_call_target="tpu_custom_call" | custom-call | flops 3500000000 | bytes 7000000 | tf_op jit(solution)/shard_map/states/pallas_call | solution.py:489
  7.9 3.1 %collective-permute-start.2 = (bf16[72,1024]{1,0:T(8,128)(2,1)}, bf16[72,1024]{1,0:T(8,128)(2,1)}, u32[]{:S(2)}, u32[]{:S(2)}) collective-permute-start(bf16[72,1024]{1,0:T(8,128)(2,1)} %states.1.own_ref), channel_id=1, source_target_pairs={{0,24},{8,0},{16,8},{24,16},{1,25},{9,1},{17,9},{25,17},{2,26},{10... | collective-permute-start | bytes 442376 | tf_op jit(solution)/shard_map/ppermute | solution.py:500
  11.1 2.8 %collective-permute-start.8 = (bf16[128,2048]{1,0:T(8,128)(2,1)S(1)}, bf16[128,2048]{1,0:T(8,128)(2,1)}, u32[]{:S(2)}, u32[]{:S(2)}) collective-permute-start(bf16[128,2048]{1,0:T(8,128)(2,1)S(1)} %copy-done.11), channel_id=1, source_target_pairs={{0,6},{2,0},{4,2},{6,4},{1,7},{3,1},{5,3},{7,5},{8,14},{10,8},{12,... | collective-permute-start | bytes 1572872 | tf_op jit(solution)/shard_map/ppermute | solution.py:484
  17.1 6.3 %collective-permute-done.1.two_ref = bf16[72,1024]{1,0:T(8,128)(2,1)} collective-permute-done((bf16[72,1024]{1,0:T(8,128)(2,1)}, bf16[72,1024]{1,0:T(8,128)(2,1)}, u32[]{:S(2)}, u32[]{:S(2)}) %collective-permute-start.1) | collective-permute-done | bytes 147488 | tf_op jit(solution)/shard_map/ppermute | solution.py:500
  23.4 1.6 collective-permute-done.one_ref
  25.0 2.1 row.1
  27.1 5.9 %collective-permute-start.5 = (bf16[72,1024]{1,0:T(8,128)(2,1)}, bf16[72,1024]{1,0:T(8,128)(2,1)S(1)}, u32[]{:S(2)}, u32[]{:S(2)}) collective-permute-start(bf16[72,1024]{1,0:T(8,128)(2,1)} %get-tuple-element.27), channel_id=1, source_target_pairs={{0,96},{1,97},{2,98},{3,99},{4,100},{5,101},{6,102},{7,103},{8,104... | collective-permute-start | bytes 442376 | tf_op jit(solution)/shard_map/ppermute | solution.py:531
  33.0 1.3 collective-permute-start.4
  34.3 1.7 collective-permute-done.8.refs_3_
  36.0 3.8 %collective-permute-done.6.refs_1_ = bf16[128,2048]{1,0:T(8,128)(2,1)} collective-permute-done((bf16[128,2048]{1,0:T(8,128)(2,1)S(1)}, bf16[128,2048]{1,0:T(8,128)(2,1)}, u32[]{:S(2)}, u32[]{:S(2)}) %collective-permute-start.6) | collective-permute-done | bytes 524320 | tf_op jit(solution)/shard_map/ppermute | solution.py:484
  40.4 4.5 %collective-permute-start.3 = (bf16[72,1024]{1,0:T(8,128)(2,1)}, bf16[72,1024]{1,0:T(8,128)(2,1)}, u32[]{:S(2)}, u32[]{:S(2)}) collective-permute-start(bf16[72,1024]{1,0:T(8,128)(2,1)} %get-tuple-element.27), channel_id=1, source_target_pairs={{0,32},{32,64},{64,96},{1,33},{33,65},{65,97},{2,34},{34,66},{66,9... | collective-permute-start | bytes 442376 | tf_op jit(solution)/shard_map/ppermute | solution.py:531
  44.9 8.3 %inside.1 = (f32[384,1024]{1,0:T(8,128)}, bf16[384,1024]{1,0:T(8,128)(2,1)}) custom-call(bf16[384,1024]{1,0:T(8,128)(2,1)} %bitcast.30, bf16[384,1024]{1,0:T(8,128)(2,1)} %bitcast.32, bf16[384,1024]{1,0:T(8,128)(2,1)} %bitcast.34, f32[1,1024]{1,0:T(1,128)} %bitcast.38, f32[16,384]{1,0:T(8,128)} %dynamic-slice_bitcast_fusion.spike_ref), custom_call_target="tpu_custom_call" | custom-call | flops 4000000000 | bytes 8000000 | tf_op jit(solution)/shard_map/inside/pallas_call | solution.py:506
  55.1 13.7 %mix.1 = (bf16[384,2048]{1,0:T(8,128)(2,1)}, bf16[1536,2048]{1,0:T(8,128)(2,1)}) custom-call(s32[3]{0:T(128)} %pad_add_fusion.pos_ref, f32[384,1024]{1,0:T(8,128)} %get-tuple-element.23.out_ref, bf16[384,1024]{1,0:T(8,128)(2,1)} %get-tuple-element.24.qrun_ref, bf16[384,1024]{1,0:T(8,128)(2,1)} %bitcast.35, bf16[384,2048]{1,0:T(8,128)(2,1)} %bitcast.29, ...), custom_call_target="tpu_custom_call" | custom-call | flops 6000000000 | bytes 12000000 | tf_op jit(solution)/shard_map/mix/pallas_call | solution.py:565
  68.8 80.2 %all_to_all.15.x_ref = bf16[16,96,2048]{2,1,0:T(8,128)(2,1)} all-to-all(bf16[16,96,2048]{2,1,0:T(8,128)(2,1)} %bitcast.26), channel_id=1, replica_groups=mesh['sp_0'=4,'sp_1'=4,'x'=4,'c'=2] {'sp_0','sp_1'}, dimensions={0} | all-to-all | bytes 12582912 | tf_op jit(solution)/shard_map/all_to_all | solution.py:604
  149.0 6.2 %serve.3 = bf16[16,16,2048]{2,1,0:T(8,128)(2,1)} custom-call(bf16[16,96,2048]{2,1,0:T(8,128)(2,1)} %all_to_all.15.x_ref, bf16[1,2048,1024]{2,1,0:T(8,128)(2,1)S(1)} %copy-done.1, bf16[1,2048,1024]{2,1,0:T(8,128)(2,1)S(1)} %copy-done.2, bf16[1,1024,2048]{2,1,0:T(8,128)(2,1)S(1)} %copy-done.3), custom_call_target="tpu_custom_call" | custom-call | flops 2500000000 | bytes 5000000 | tf_op jit(solution)/shard_map/serve/pallas_call | solution.py:612
  155.2 3.7 %all-to-all-start.2 = ((bf16[16,16,2048]{2,1,0:T(8,128)(2,1)}), bf16[16,16,2048]{2,1,0:T(8,128)(2,1)S(1)}, u32[]{:S(2)}, u32[]{:S(2)}) async-start(bf16[16,16,2048]{2,1,0:T(8,128)(2,1)} %serve.3), calls=%async_computation.2 | async-start | bytes 2097152 | tf_op jit(solution)/shard_map/all_to_all | solution.py:604
  158.9 21.6 %serve.2 = bf16[16,80,2048]{2,1,0:T(8,128)(2,1)} custom-call(bf16[16,96,2048]{2,1,0:T(8,128)(2,1)} %all_to_all.15.x_ref, bf16[1,2048,1024]{2,1,0:T(8,128)(2,1)} %wg_ref.3, bf16[1,2048,1024]{2,1,0:T(8,128)(2,1)} %wu_ref.3, bf16[1,1024,2048]{2,1,0:T(8,128)(2,1)} %wd_ref.3), custom_call_target="tpu_custom_call" | custom-call | flops 10000000000 | bytes 20000000 | tf_op jit(solution)/shard_map/serve/pallas_call | solution.py:612
  181.4 7.2 %all-to-all-start.1 = ((bf16[16,80,2048]{2,1,0:T(8,128)(2,1)}), bf16[16,80,2048]{2,1,0:T(8,128)(2,1)}, u32[]{:S(2)}, u32[]{:S(2)}) async-start(bf16[16,80,2048]{2,1,0:T(8,128)(2,1)} %serve.2), calls=%async_computation.1 | async-start | bytes 10485760 | tf_op jit(solution)/shard_map/all_to_all | solution.py:604
  188.6 3.2 %weights.1 = (bf16[384,1280]{1,0:T(8,128)(2,1)}, bf16[384,256]{1,0:T(8,128)(2,1)}) custom-call(s32[8,384]{1,0:T(8,128)} %pad.8.routes_ref.refs_9_, f32[8,384]{1,0:T(8,128)} %pad.9.wt_ref), custom_call_target="tpu_custom_call" | custom-call | flops 1000000000 | bytes 2000000 | tf_op jit(solution)/shard_map/weights/pallas_call | solution.py:540
  191.8 72.7 %all-to-all-done.1 = bf16[16,80,2048]{2,1,0:T(8,128)(2,1)} async-done(((bf16[16,80,2048]{2,1,0:T(8,128)(2,1)}), bf16[16,80,2048]{2,1,0:T(8,128)(2,1)}, u32[]{:S(2)}, u32[]{:S(2)}) %all-to-all-start.1) | async-done | bytes 5242912 | tf_op jit(solution)/shard_map/all_to_all | solution.py:604
  264.5 1.2 copy-done.5
  265.7 1.4 copy-done.6
  267.1 1.2 copy-done.7
  269.3 5.9 %combine.1 = bf16[384,2048]{1,0:T(8,128)(2,1)} custom-call(bf16[384,1280]{1,0:T(8,128)(2,1)S(1)} %copy-done.7, bf16[384,256]{1,0:T(8,128)(2,1)S(1)} %copy-done.8, bf16[1280,2048]{1,0:T(8,128)(2,1)} %bitcast.19.got_ref, bf16[256,2048]{1,0:T(8,128)(2,1)S(1)} %bitcast.25, bf16[384,2048]{1,0:T(8,128)(2,1)S(1)} %copy-done.6), custom_call_target="tpu_custom_call" | custom-call | flops 2000000000 | bytes 4000000 | tf_op jit(solution)/shard_map/combine/pallas_call | solution.py:644
  (47 shorter events, 9.3 us)
Async XLA Ops:
  1.6 9.5 %copy-start.11 = (bf16[128,2048]{1,0:T(8,128)(2,1)S(1)}, bf16[128,2048]{1,0:T(8,128)(2,1)}, u32[]{:S(2)}) copy-start(bf16[128,2048]{1,0:T(8,128)(2,1)} %refs_0_.1) | copy-start | bytes 1572868
  7.9 8.2 %collective-permute-start.2 = (bf16[72,1024]{1,0:T(8,128)(2,1)}, bf16[72,1024]{1,0:T(8,128)(2,1)}, u32[]{:S(2)}, u32[]{:S(2)}) collective-permute-start(bf16[72,1024]{1,0:T(8,128)(2,1)} %states.1.own_ref), channel_id=1, source_target_pairs={{0,24},{8,0},{16,8},{24,16},{1,25},{9,1},{17,9},{25,17},{2,26},{10... | collective-permute-start | bytes 442376 | tf_op jit(solution)/shard_map/ppermute | solution.py:500
  11.1 24.9 %collective-permute-start.8 = (bf16[128,2048]{1,0:T(8,128)(2,1)S(1)}, bf16[128,2048]{1,0:T(8,128)(2,1)}, u32[]{:S(2)}, u32[]{:S(2)}) collective-permute-start(bf16[128,2048]{1,0:T(8,128)(2,1)S(1)} %copy-done.11), channel_id=1, source_target_pairs={{0,6},{2,0},{4,2},{6,4},{1,7},{3,1},{5,3},{7,5},{8,14},{10,8},{12,... | collective-permute-start | bytes 1572872 | tf_op jit(solution)/shard_map/ppermute | solution.py:484
  13.8 22.2 %collective-permute-start.7 = (bf16[128,2048]{1,0:T(8,128)(2,1)S(1)}, bf16[128,2048]{1,0:T(8,128)(2,1)}, u32[]{:S(2)}, u32[]{:S(2)}) collective-permute-start(bf16[128,2048]{1,0:T(8,128)(2,1)S(1)} %copy-done.11), channel_id=1, source_target_pairs={{0,4},{2,6},{4,0},{6,2},{1,5},{3,7},{5,1},{7,3},{8,12},{10,14},{12... | collective-permute-start | bytes 1572872 | tf_op jit(solution)/shard_map/ppermute | solution.py:484
  14.6 25.1 %collective-permute-start.6 = (bf16[128,2048]{1,0:T(8,128)(2,1)S(1)}, bf16[128,2048]{1,0:T(8,128)(2,1)}, u32[]{:S(2)}, u32[]{:S(2)}) collective-permute-start(bf16[128,2048]{1,0:T(8,128)(2,1)S(1)} %copy-done.11), channel_id=1, source_target_pairs={{0,2},{2,4},{4,6},{6,0},{1,3},{3,5},{5,7},{7,1},{8,10},{10,12},{12... | collective-permute-start | bytes 1572872 | tf_op jit(solution)/shard_map/ppermute | solution.py:484
  15.5 7.9 %collective-permute-start.1 = (bf16[72,1024]{1,0:T(8,128)(2,1)}, bf16[72,1024]{1,0:T(8,128)(2,1)}, u32[]{:S(2)}, u32[]{:S(2)}) collective-permute-start(bf16[72,1024]{1,0:T(8,128)(2,1)} %states.1.own_ref), channel_id=1, source_target_pairs={{0,16},{8,24},{16,0},{24,8},{1,17},{9,25},{17,1},{25,9},{2,18},{10... | collective-permute-start | bytes 442376 | tf_op jit(solution)/shard_map/ppermute | solution.py:500
  16.1 8.8 %collective-permute-start = (bf16[72,1024]{1,0:T(8,128)(2,1)}, bf16[72,1024]{1,0:T(8,128)(2,1)}, u32[]{:S(2)}, u32[]{:S(2)}) collective-permute-start(bf16[72,1024]{1,0:T(8,128)(2,1)} %states.1.own_ref), channel_id=1, source_target_pairs={{0,8},{8,16},{16,24},{24,0},{1,9},{9,17},{17,25},{25,1},{2,10},{10... | collective-permute-start | bytes 442376 | tf_op jit(solution)/shard_map/ppermute | solution.py:500
  27.1 13.2 %collective-permute-start.5 = (bf16[72,1024]{1,0:T(8,128)(2,1)}, bf16[72,1024]{1,0:T(8,128)(2,1)S(1)}, u32[]{:S(2)}, u32[]{:S(2)}) collective-permute-start(bf16[72,1024]{1,0:T(8,128)(2,1)} %get-tuple-element.27), channel_id=1, source_target_pairs={{0,96},{1,97},{2,98},{3,99},{4,100},{5,101},{6,102},{7,103},{8,104... | collective-permute-start | bytes 442376 | tf_op jit(solution)/shard_map/ppermute | solution.py:531
  33.0 7.4 %collective-permute-start.4 = (bf16[72,1024]{1,0:T(8,128)(2,1)}, bf16[72,1024]{1,0:T(8,128)(2,1)S(1)}, u32[]{:S(2)}, u32[]{:S(2)}) collective-permute-start(bf16[72,1024]{1,0:T(8,128)(2,1)} %get-tuple-element.27), channel_id=1, source_target_pairs={{0,64},{32,96},{1,65},{33,97},{2,66},{34,98},{3,67},{35,99},{4,68}... | collective-permute-start | bytes 442376 | tf_op jit(solution)/shard_map/ppermute | solution.py:531
  36.0 19.0 %collective-permute-start.9 = (bf16[128,2048]{1,0:T(8,128)(2,1)S(1)}, bf16[128,2048]{1,0:T(8,128)(2,1)}, u32[]{:S(2)}, u32[]{:S(2)}) collective-permute-start(bf16[128,2048]{1,0:T(8,128)(2,1)S(1)} %copy-done.11), channel_id=1, source_target_pairs={{0,1},{1,0},{2,3},{3,2},{4,5},{5,4},{6,7},{7,6},{8,9},{9,8},{10,11... | collective-permute-start | bytes 1572872 | tf_op jit(solution)/shard_map/ppermute | solution.py:535
  39.8 15.3 %collective-permute-start.10 = (bf16[128,2048]{1,0:T(8,128)(2,1)}, bf16[128,2048]{1,0:T(8,128)(2,1)}, u32[]{:S(2)}, u32[]{:S(2)}) collective-permute-start(bf16[128,2048]{1,0:T(8,128)(2,1)} %collective-permute-done.6.refs_1_), channel_id=1, source_target_pairs={{0,1},{1,0},{2,3},{3,2},{4,5},{5,4},{6,7},{7,6},{8,9},{9,8},{10,11... | collective-permute-start | bytes 1572872 | tf_op jit(solution)/shard_map/ppermute | solution.py:535
  39.8 15.3 %collective-permute-start.11 = (bf16[128,2048]{1,0:T(8,128)(2,1)}, bf16[128,2048]{1,0:T(8,128)(2,1)}, u32[]{:S(2)}, u32[]{:S(2)}) collective-permute-start(bf16[128,2048]{1,0:T(8,128)(2,1)} %collective-permute-done.7.refs_2_), channel_id=1, source_target_pairs={{0,1},{1,0},{2,3},{3,2},{4,5},{5,4},{6,7},{7,6},{8,9},{9,8},{10,11... | collective-permute-start | bytes 1572872 | tf_op jit(solution)/shard_map/ppermute | solution.py:535
  40.3 4.6 %copy-start.12 = (bf16[72,1024]{1,0:T(8,128)(2,1)}, bf16[72,1024]{1,0:T(8,128)(2,1)S(1)}, u32[]{:S(2)}) copy-start(bf16[72,1024]{1,0:T(8,128)(2,1)S(1)} %collective-permute-done.5.three_ref) | copy-start | bytes 442372
  40.3 14.8 %collective-permute-start.12 = (bf16[128,2048]{1,0:T(8,128)(2,1)}, bf16[128,2048]{1,0:T(8,128)(2,1)}, u32[]{:S(2)}, u32[]{:S(2)}) collective-permute-start(bf16[128,2048]{1,0:T(8,128)(2,1)} %collective-permute-done.8.refs_3_), channel_id=1, source_target_pairs={{0,1},{1,0},{2,3},{3,2},{4,5},{5,4},{6,7},{7,6},{8,9},{9,8},{10,11... | collective-permute-start | bytes 1572872 | tf_op jit(solution)/shard_map/ppermute | solution.py:535
  40.4 4.5 %copy-start.13 = (bf16[72,1024]{1,0:T(8,128)(2,1)}, bf16[72,1024]{1,0:T(8,128)(2,1)S(1)}, u32[]{:S(2)}) copy-start(bf16[72,1024]{1,0:T(8,128)(2,1)S(1)} %collective-permute-done.4.two_ref) | copy-start | bytes 442372
  40.4 14.7 %collective-permute-start.3 = (bf16[72,1024]{1,0:T(8,128)(2,1)}, bf16[72,1024]{1,0:T(8,128)(2,1)}, u32[]{:S(2)}, u32[]{:S(2)}) collective-permute-start(bf16[72,1024]{1,0:T(8,128)(2,1)} %get-tuple-element.27), channel_id=1, source_target_pairs={{0,32},{32,64},{64,96},{1,33},{33,65},{65,97},{2,34},{34,66},{66,9... | collective-permute-start | bytes 442376 | tf_op jit(solution)/shard_map/ppermute | solution.py:531
  44.9 8.3 %copy-start.9 = (s32[1,384,2]{1,2,0:T(2,128)S(1)}, s32[1,384,2]{1,2,0:T(2,128)}, u32[]{:S(2)}) copy-start(s32[1,384,2]{1,2,0:T(2,128)} %param.26) | copy-start | bytes 9220
  44.9 8.9 %copy-start.10 = (f32[1,384,2]{1,2,0:T(2,128)S(1)}, f32[1,384,2]{1,2,0:T(2,128)}, u32[]{:S(2)}) copy-start(f32[1,384,2]{1,2,0:T(2,128)} %param.27) | copy-start | bytes 9220
  68.8 80.3 %copy-start.1 = (bf16[1,2048,1024]{2,1,0:T(8,128)(2,1)S(1)}, bf16[1,2048,1024]{2,1,0:T(8,128)(2,1)}, u32[]{:S(2)}) copy-start(bf16[1,2048,1024]{2,1,0:T(8,128)(2,1)} %wg_ref.3) | copy-start | bytes 12582916
  68.8 80.3 %copy-start.2 = (bf16[1,2048,1024]{2,1,0:T(8,128)(2,1)S(1)}, bf16[1,2048,1024]{2,1,0:T(8,128)(2,1)}, u32[]{:S(2)}) copy-start(bf16[1,2048,1024]{2,1,0:T(8,128)(2,1)} %wu_ref.3) | copy-start | bytes 12582916
  68.8 80.2 %copy-start.3 = (bf16[1,1024,2048]{2,1,0:T(8,128)(2,1)S(1)}, bf16[1,1024,2048]{2,1,0:T(8,128)(2,1)}, u32[]{:S(2)}) copy-start(bf16[1,1024,2048]{2,1,0:T(8,128)(2,1)} %wd_ref.3) | copy-start | bytes 12582916
  155.2 25.3 %all-to-all-start.2 = ((bf16[16,16,2048]{2,1,0:T(8,128)(2,1)}), bf16[16,16,2048]{2,1,0:T(8,128)(2,1)S(1)}, u32[]{:S(2)}, u32[]{:S(2)}) async-start(bf16[16,16,2048]{2,1,0:T(8,128)(2,1)} %serve.3), calls=%async_computation.2 | async-start | bytes 2097152 | tf_op jit(solution)/shard_map/all_to_all | solution.py:604
  181.4 83.1 %all-to-all-start.1 = ((bf16[16,80,2048]{2,1,0:T(8,128)(2,1)}), bf16[16,80,2048]{2,1,0:T(8,128)(2,1)}, u32[]{:S(2)}, u32[]{:S(2)}) async-start(bf16[16,80,2048]{2,1,0:T(8,128)(2,1)} %serve.2), calls=%async_computation.1 | async-start | bytes 10485760 | tf_op jit(solution)/shard_map/all_to_all | solution.py:604
  265.7 1.4 copy-start.6
  (5 other events, 5.3 us)
